TPU v7x, 256 devices: a whole 4x4x8 slice. The times are simulated.
256 devices in a mesh: sp: 64 (over z, x, core), tp: 4 (over y).
Axes of the slice: x: 4, y: 4, z: 8, core: 2. Of those that a mesh axis runs over, the one named last changes fastest.
Arguments:
- residual: bfloat16 [32768, 2048], P(('sp', 'tp')), may hold values from -6 to 6
- queries: bfloat16 [32768, 1024], P('sp', 'tp'), may hold values from -6 to 6
- key_vectors: bfloat16 [32768, 1024], P('sp', 'tp'), may hold values from -6 to 6
- value_vectors: bfloat16 [32768, 1024], P('sp', 'tp'), may hold values from -6 to 6
- output_gate: bfloat16 [32768, 1024], P('sp', 'tp'), may hold values from -6 to 6
- input_gate: float32 [32768, 16], P('sp', 'tp'), may hold values from -4 to 250
- forget_gate: float32 [32768, 16], P('sp', 'tp'), may hold values from 0 to 20
- head_gain: float32 [16, 64], P('tp'), may hold values from 0.1 to 1.9
- output_weight: bfloat16 [1024, 2048], replicated, may hold values from -0.1875 to 0.1875
- norm_gain: float32 [2048], replicated, may hold values from 0.1 to 1.9
- route_experts: int32 [32768, 2], P('sp'), may hold values from 0 to 63, as said below
- group_weight: float32 [32768], P('sp'), may hold values from 0.25 to 1
- expert_scores: float32 [32768, 2], P('sp'), may hold values from -6 to 6
- gate_weight: bfloat16 [64, 2048, 1024], P('sp', None, 'tp'), may hold values from -0.125 to 0.125
- up_weight: bfloat16 [64, 2048, 1024], P('sp', None, 'tp'), may hold values from -0.125 to 0.125
- down_weight: bfloat16 [64, 1024, 2048], P('sp', 'tp'), may hold values from -0.1875 to 0.1875
Outputs:
- mixed_out: bfloat16 [32768, 2048], P(('sp', 'tp'))
Inputs may be any that keep to these rules, and one draw needn't show every extreme that they name: `route_experts`: the two experts of a row differ and lie in the same group of 16 consecutive experts. In each aligned block of 128 rows no expert is named more than 8 times, and in every block some expert is named exactly 8 times.
All inputs are finite; a program needn't handle non-finite values.
Results may differ from a plain program's by a relative error of at most 0.012.
Values may be sent and summed in bfloat16 or wider, within the bound.
A program may use at most 128 MiB of HBM per device.

v0:
```python
import jax
import jax.numpy as jnp
from jax import lax
from jax.sharding import Mesh
from jax.sharding import PartitionSpec as P

TOP = 2
BLOCK = 128
SP = ("sp_0", "sp_1", "sp_2")
SP_TP = ("sp_0", "sp_1", "sp_2", "tp")


EPSILON = 1e-06
VERY_NEGATIVE = -1e30
PRECISE = lax.Precision.HIGHEST


def turned_gather(arrays, axis, dims):
    turned = [jnp.moveaxis(a, dim, 0) for a, dim in zip(arrays, dims)]
    widths = [t[0].size for t in turned]
    both = jnp.concatenate([t.reshape(-1, w) for t, w in zip(turned, widths)], axis=1)
    whole = lax.all_gather(both, axis, axis=0, tiled=True)
    tiles = jnp.split(whole, [sum(widths[:k]) for k in range(1, len(widths))], axis=1)
    return tuple(
        (
            jnp.moveaxis(b.reshape(-1, *t.shape[1:]), 0, dim)
            for b, t, dim in zip(tiles, turned, dims)
        )
    )


def neutral_like(value, identity):
    return jax.tree.map(
        lambda part, zero: jnp.zeros_like(part) + jnp.asarray(zero, part.dtype), value, identity
    )


def gathered_once(value, axis):
    leaves = jax.tree.leaves(value)
    turns = sorted(range(len(leaves)), key=lambda k: -leaves[k].size)
    width = (1, *leaves[turns[0]].shape)[-1]
    lines = [
        jnp.pad(leaves[k].reshape(-1), (0, -leaves[k].size % width)).reshape(-1, width)
        for k in turns
    ]
    both, at, found = (lax.all_gather(jnp.concatenate(lines), axis), 0, {})
    for k, line in zip(turns, lines):
        section = both[:, at : at + len(line)].reshape(len(both), -1)
        found[k] = section[:, : leaves[k].size].reshape(-1, *leaves[k].shape)
        at += len(line)
    numbers = iter(range(len(leaves)))
    return jax.tree.map(lambda _: found[next(numbers)], value)


def entering(value, axes, combine, identity):
    before = start = neutral_like(value, identity)
    subtotal = value
    for axis in reversed(axes):
        peers, here = (lax.axis_size(axis), lax.axis_index(axis))
        pieces = gathered_once(subtotal, axis)
        inside, subtotal = (start, start)
        for k in range(peers):
            passed = k < here
            subtotal = combine(subtotal, jax.tree.map(lambda part: part[k], pieces))
            inside = jax.tree.map(lambda new, old: jnp.where(passed, new, old), subtotal, inside)
        before = combine(inside, before)
    return before


def block_step(carried, pieces):
    memory, stabilizer = carried
    query_block, key_block, value_block, decay_block, gate_block = pieces
    block_size = query_block.shape[0]
    causal_mask = jnp.tril(jnp.ones((block_size, block_size), dtype=bool))
    decay_rows = decay_block.T
    gate_rows = gate_block.T
    pair_log = decay_rows[:, :, None] - decay_rows[:, None, :] + gate_rows[:, None, :]
    pair_log = jnp.where(causal_mask[None], pair_log, -jnp.inf)
    carry_log = decay_rows + stabilizer[:, None]
    peak_level = jnp.maximum(carry_log, jnp.max(pair_log, axis=-1))
    within_weight = jnp.exp(pair_log - peak_level[:, :, None])
    carry_weight = jnp.exp(carry_log - peak_level)
    scores = jnp.einsum("thd,shd->hts", query_block, key_block, precision=PRECISE) * within_weight
    numerator = jnp.einsum("hts,shd->htd", scores, value_block, precision=PRECISE)
    numerator = numerator + carry_weight[:, :, None] * jnp.einsum(
        "thd,hde->hte", query_block, memory, precision=PRECISE
    )
    outputs = jnp.transpose(numerator, (1, 0, 2))
    final_decay = decay_rows[:, -1]
    key_log = final_decay[:, None] - decay_rows + gate_rows
    new_level = jnp.maximum(final_decay + stabilizer, jnp.max(key_log, axis=-1))
    key_weight = jnp.exp(key_log - new_level[:, None])
    carry_fade = jnp.exp(final_decay + stabilizer - new_level)
    memory = carry_fade[:, None, None] * memory + jnp.einsum(
        "hs,shd,she->hde", key_weight, key_block, value_block, precision=PRECISE
    )
    return ((memory, new_level), outputs)


def cell_outputs(query_part, key_part, value_part, input_gate, log_forget, initial):
    length, head_count, head_size = query_part.shape
    block_count = length // BLOCK
    cumulative = jnp.cumsum(log_forget.reshape(block_count, BLOCK, head_count), axis=1)
    shaped = (
        query_part.reshape(block_count, BLOCK, head_count, head_size),
        key_part.reshape(block_count, BLOCK, head_count, head_size),
        value_part.reshape(block_count, BLOCK, head_count, head_size),
        cumulative,
        input_gate.reshape(block_count, BLOCK, head_count),
    )
    _, outputs = lax.scan(block_step, initial, shaped)
    return outputs.reshape(length, head_count, head_size)


def chain_join(earlier, latter):
    early_total, early_level, early_memory = earlier
    late_total, late_level, late_memory = latter
    joined_level = jnp.maximum(late_total + early_level, late_level)
    fade_early = jnp.exp(late_total + early_level - joined_level)
    fade_late = jnp.exp(late_level - joined_level)
    joined_memory = (
        fade_early[:, None, None] * early_memory + fade_late[:, None, None] * late_memory
    )
    return (early_total + late_total, joined_level, joined_memory)


def slot_within(flat_routes, expert_total):
    onehot = (flat_routes[:, None] == jnp.arange(expert_total, dtype=jnp.int32)[None, :]).astype(
        jnp.int32
    )
    before = jnp.cumsum(onehot, axis=0) - onehot
    return jnp.sum(before * onehot, axis=1)


def fill_slots(source_rows, places, slot_total):
    assign = jnp.arange(places.shape[0], dtype=jnp.int32) // TOP
    owner_index = jnp.full((slot_total,), source_rows.shape[0], jnp.int32).at[places].set(assign)
    padded = jnp.concatenate(
        [source_rows, jnp.zeros((1, source_rows.shape[1]), source_rows.dtype)], axis=0
    )
    return padded[owner_index]


def expert_whole(chosen_rows, whole_gate, whole_up, whole_down, part_count):
    gate_value = jnp.dot(chosen_rows, whole_gate[0], preferred_element_type=jnp.float32)
    up_value = jnp.dot(chosen_rows, whole_up[0], preferred_element_type=jnp.float32)
    hidden = (jax.nn.silu(gate_value) * up_value).astype(jnp.bfloat16)
    part_width = hidden.shape[1] // part_count
    summed = jnp.zeros((chosen_rows.shape[0], whole_down.shape[2]), jnp.float32)
    for quarter in range(part_count):
        piece_out = jnp.dot(
            hidden[:, quarter * part_width : (quarter + 1) * part_width],
            whole_down[0, quarter * part_width : (quarter + 1) * part_width],
            preferred_element_type=jnp.float32,
        ).astype(jnp.bfloat16)
        summed = summed + piece_out.astype(jnp.float32)
    return summed


def shards(
    residual,
    queries,
    key_vectors,
    value_vectors,
    output_gate,
    input_gate,
    forget_gate,
    head_gain,
    output_weight,
    norm_gain,
    route_experts,
    group_weight,
    expert_scores,
    gate_weight,
    up_weight,
    down_weight,
):
    local_length, mixer_width = queries.shape
    head_count = input_gate.shape[1]
    head_size = mixer_width // head_count
    token_count, model_width = residual.shape
    token_block = lax.axis_index("tp")
    whole_gate, whole_up, whole_down = turned_gather(
        (gate_weight, up_weight, down_weight), "tp", (2, 2, 1)
    )
    query_part = queries.astype(jnp.float32).reshape(
        local_length, head_count, head_size
    ) * head_size ** (-0.5)
    key_part = key_vectors.astype(jnp.float32).reshape(local_length, head_count, head_size)
    value_part = value_vectors.astype(jnp.float32).reshape(local_length, head_count, head_size)
    log_forget = jax.nn.log_sigmoid(forget_gate)
    running = jnp.cumsum(log_forget, axis=0)
    log_total = running[-1]
    key_log = log_total[None, :] - running + input_gate
    local_level = jnp.max(key_log, axis=0)
    key_weight = jnp.exp(key_log - local_level[None, :])
    local_memory = jnp.einsum(
        "sh,shd,she->hde", key_weight, key_part, value_part, precision=PRECISE
    )
    identity = (
        jnp.zeros_like(log_total),
        jnp.full_like(local_level, VERY_NEGATIVE),
        jnp.zeros_like(local_memory),
    )
    prior_total, prior_level, prior_memory = entering(
        (log_total, local_level, local_memory), SP, chain_join, identity
    )
    start_level = jnp.maximum(prior_level, prior_total)
    opening_decay = jnp.exp(prior_level - start_level)
    initial = (opening_decay[:, None, None] * prior_memory, start_level)
    cell_out = cell_outputs(query_part, key_part, value_part, input_gate, log_forget, initial)
    normed_heads = (
        cell_out
        * lax.rsqrt(jnp.mean(cell_out * cell_out, axis=-1, keepdims=True) + EPSILON)
        * head_gain
    )
    mixed_rows = (
        jax.nn.sigmoid(output_gate.astype(jnp.float32))
        * normed_heads.reshape(local_length, mixer_width)
    ).astype(jnp.bfloat16)
    token_major = lax.all_to_all(mixed_rows, "tp", split_axis=0, concat_axis=1, tiled=True)
    projected = jnp.dot(token_major, output_weight, preferred_element_type=jnp.float32)
    stream_float = (
        (residual.astype(jnp.float32) + projected).astype(jnp.bfloat16).astype(jnp.float32)
    )
    normed = (
        stream_float
        * lax.rsqrt(jnp.mean(stream_float * stream_float, axis=-1, keepdims=True) + EPSILON)
        * norm_gain
    ).astype(jnp.bfloat16)
    expert_total = lax.axis_size(SP)
    group_size = lax.axis_size("tp")
    capacity = 2 * TOP * token_count // expert_total
    own_routes = lax.dynamic_slice_in_dim(
        route_experts, token_block * token_count, token_count, 0
    ).reshape(-1)
    own_group = lax.dynamic_slice_in_dim(group_weight, token_block * token_count, token_count, 0)
    own_scores = lax.dynamic_slice_in_dim(expert_scores, token_block * token_count, token_count, 0)
    own_places = own_routes * capacity + slot_within(own_routes, expert_total)
    send_rows = fill_slots(normed, own_places, expert_total * capacity)
    arrived = lax.all_to_all(
        send_rows.reshape(expert_total, capacity, model_width),
        SP,
        split_axis=0,
        concat_axis=0,
        tiled=True,
    )
    returned = expert_whole(
        arrived.reshape(expert_total * capacity, model_width),
        whole_gate,
        whole_up,
        whole_down,
        group_size,
    )
    answers = lax.all_to_all(
        returned.reshape(expert_total, capacity, model_width).astype(jnp.bfloat16),
        SP,
        split_axis=0,
        concat_axis=0,
        tiled=True,
    )
    picked = (
        answers.reshape(expert_total * capacity, model_width)[own_places]
        .astype(jnp.float32)
        .reshape(token_count, TOP, model_width)
    )
    route_weight = own_group[:, None] * jax.nn.softmax(own_scores, axis=-1)
    expert_mix = jnp.sum(picked * route_weight[:, :, None], axis=1)
    return (stream_float + expert_mix).astype(jnp.bfloat16)


def solution(mesh):
    finer = Mesh(mesh.devices.reshape(8, 4, 2, mesh.shape["tp"]), ("sp_0", "sp_1", "sp_2", "tp"))
    return jax.shard_map(
        shards,
        mesh=finer,
        in_specs=(
            P(SP_TP, None),
            P(SP, "tp"),
            P(SP, "tp"),
            P(SP, "tp"),
            P(SP, "tp"),
            P(SP, "tp"),
            P(SP, "tp"),
            P("tp", None),
            P(),
            P(),
            P(SP, None),
            P(SP),
            P(SP, None),
            P(SP, None, "tp"),
            P(SP, None, "tp"),
            P(SP, "tp", None),
        ),
        out_specs=P(SP_TP, None),
        check_vma=False,
    )
```

profile of v0, /device:TPU:1, one launch (start us, length us, event | category | flops | bytes accessed | tf_op | source)
XLA Modules:
  0.0 264.6 jit_solution(17445495401705264585)
XLA Ops:
  6.5 1.6 copy.208
  8.1 1.5 copy.209
  9.6 1.8 pad_maximum_fusion
  12.2 1.2 reduce-window.14
  16.1 4.8 %all-gather.3 = f32[2,258,64]{1,2,0:T(8,128)S(1)} all-gather(f32[1,258,64]{1,2,0:T(8,128)S(1)} %maximum_bitcast_fusion), channel_id=2, replica_groups=mesh['sp_0'=8,'sp_1'=4,'sp_2'=2,'tp'=4] {'sp_2'}, dimensions={0}, use_global_device_ids=true | all-gather | bytes 198144 | tf_op jit(solution)/shard_map/all_gather | solution.py:46
  22.1 9.6 %all-gather.4 = f32[4,258,64]{1,2,0:T(8,128)S(1)} all-gather(f32[1,258,64]{1,2,0:T(8,128)S(1)} %maximum_bitcast_fusion.1), channel_id=3, replica_groups=mesh['sp_0'=8,'sp_1'=4,'sp_2'=2,'tp'=4] {'sp_1'}, dimensions={0}, use_global_device_ids=true | all-gather | bytes 330240 | tf_op jit(solution)/shard_map/all_gather | solution.py:46
  34.4 25.2 %all-gather.5 = f32[8,258,64]{1,2,0:T(8,128)S(1)} all-gather(f32[1,258,64]{1,2,0:T(8,128)S(1)} %maximum_bitcast_fusion.2), channel_id=4, replica_groups=mesh['sp_0'=8,'sp_1'=4,'sp_2'=2,'tp'=4] {'sp_0'}, dimensions={0}, use_global_device_ids=true | all-gather | bytes 594432 | tf_op jit(solution)/shard_map/all_gather | solution.py:46
  59.6 0.8 fusion.86
  60.4 1.1 copy.232
  62.5 0.9 copy.214
  63.4 1.6 copy.215
  65.0 1.6 copy.216
  66.6 0.8 copy.217
  67.4 0.8 copy.218
  68.1 0.7 copy.219
  68.9 0.8 copy.220
  69.7 0.7 copy.221
  70.4 0.8 copy.222
  71.1 0.7 copy.223
  71.9 0.7 copy.224
  72.6 0.8 copy.225
  73.4 1.0 convert_multiply_fusion
  75.5 0.7 fusion.55
  76.8 0.7 subtract_exponential_fusion.15
  77.5 2.0 add_multiply_fusion
  79.5 12.1 %while.14 = (s32[]{:T(128)}, f32[4,64,64]{2,1,0:T(8,128)S(1)}, f32[4]{0:T(128)S(1)}, f32[4,128,4,64]{1,3,2,0:T(8,128)S(1)}, f32[4,128,4]{1,2,0:T(4,128)S(1)}, /*...) while((s32[]{:T(128)}, f32[4,64,64]{2,1,0:T(8,128)S(1)}, ...), condition=%wide.region_7.8_spmd, body=%wide.region_4.7_spmd.sunk | while | flops 151737344 | bytes 2389877 | solution.py:111
  92.5 0.7 copy_bitcast_fusion
  93.3 4.0 %all-to-all-start = ((bf16[4,128,256]{1,2,0:T(8,128)(2,1)}), bf16[4,128,256]{1,2,0:T(8,128)(2,1)S(1)}, u32[]{:S(2)}, u32[]{:S(2)}) async-start(bf16[4,128,256]{1,2,0:T(8,128)(2,1)} %copy_bitcast_fusion), calls=%async_computation | async-start | bytes 524288 | tf_op jit(solution)/shard_map/all_to_all | solution.py:221
  99.6 1.6 scatter_custom_fusion
  101.2 4.6 %all-to-all-done = bf16[4,128,256]{1,2,0:T(8,128)(2,1)S(1)} async-done(((bf16[4,128,256]{1,2,0:T(8,128)(2,1)}), bf16[4,128,256]{1,2,0:T(8,128)(2,1)S(1)}, u32[]{:S(2)}, u32[]{:S(2)}) %all-to-all-start) | async-done | bytes 262176 | tf_op jit(solution)/shard_map/all_to_all | solution.py:221
  105.8 3.1 %multiply_reduce_fusion.1 = (f32[128]{0:T(128)S(1)}, f32[128,2048]{1,0:T(8,128)S(1)}) fusion(bf16[128,1024]{0,1:T(8,128)(2,1)S(1)} %bitcast.541, bf16[1024,2048]{1,0:T(8,128)(2,1)} %param.26, bf16[128,2048]{1,0:T(8,128)(2,1)S(1)} %copy-done.4), kind=kOutput, calls=%fused_computation.66 | convolution fusion | flops 538443648 | bytes 6029824 | tf_op jit(solution)/shard_map/dot_general | solution.py:222
  109.1 3.3 %gather_fusion = bf16[512,2048]{1,0:T(8,128)(2,1)} fusion(bf16[129,2048]{1,0:T(8,128)(2,1)S(1)} %concatenate.18, s32[1024]{0:T(1024)S(1)} %pad_clamp_fusion.1), kind=kCustom, calls=%fused_computation | custom fusion | bytes 4196352 | tf_op jit(solution)/shard_map/gather | solution.py:141
  112.4 15.7 %all-to-all-start.1 = ((bf16[64,8,2048]{2,1,0:T(8,128)(2,1)}), bf16[64,8,2048]{2,1,0:T(8,128)(2,1)S(1)}, u32[]{:S(2)}, u32[]{:S(2)}) async-start(bf16[64,8,2048]{2,1,0:T(8,128)(2,1)} %bitcast.536), calls=%async_computation.1 | async-start | bytes 4194304 | tf_op jit(solution)/shard_map/all_to_all | solution.py:241
  128.2 11.0 %all-gather.8.cloned.1.call-done = bf16[1024,6144]{1,0:T(8,128)(2,1)} async-done(((bf16[256,6144]{1,0:T(8,128)(2,1)}), bf16[1024,6144]{1,0:T(8,128)(2,1)}) %all-gather.8.cloned.1.call-update) | async-done | bytes 12582928 | tf_op jit(solution)/shard_map/all_gather | solution.py:22
  139.1 4.7 %slice_bitcast_fusion = bf16[1,1024,2048]{2,1,0:T(8,128)(2,1)} fusion(bf16[1024,6144]{1,0:T(8,128)(2,1)} %all-gather.8.cloned.1.call-done), kind=kLoop, calls=%fused_computation.41 | loop fusion | bytes 8388608 | tf_op jit(solution)/shard_map/transpose;reshape | solution.py:26
  143.9 34.0 %all-to-all-done.1 = bf16[64,8,2048]{2,1,0:T(8,128)(2,1)S(1)} async-done(((bf16[64,8,2048]{2,1,0:T(8,128)(2,1)}), bf16[64,8,2048]{2,1,0:T(8,128)(2,1)S(1)}, u32[]{:S(2)}, u32[]{:S(2)}) %all-to-all-start.1) | async-done | bytes 2097184 | tf_op jit(solution)/shard_map/all_to_all | solution.py:241
  177.9 4.5 %fusion.23 = f32[512,1024]{1,0:T(8,128)S(1)} fusion(bf16[1024,6144]{1,0:T(8,128)(2,1)} %all-gather.8.cloned.1.call-done, bf16[64,8,2048]{2,1,0:T(8,128)(2,1)S(1)} %all-to-all-done.1), kind=kOutput, calls=%fused_computation.45 | convolution fusion | flops 2147483648 | bytes 8388608 | tf_op jit(solution)/shard_map/dot_general | solution.py:145
  182.4 4.9 %multiply_convert_fusion = bf16[512,1024]{1,0:T(8,128)(2,1)S(1)} fusion(f32[512,1024]{1,0:T(8,128)S(1)} %fusion.23, bf16[1024,6144]{1,0:T(8,128)(2,1)} %all-gather.8.cloned.1.call-done, bf16[64,8,2048]{2,1,0:T(8,128)(2,1)S(1)} %all-to-all-done.1), kind=kOutput, calls=%fused_computation.59 | convolution fusion | flops 2150629376 | bytes 9437184 | tf_op jit(solution)/shard_map/dot_general | solution.py:146
  188.1 0.7 convolution_convert_fusion.1
  188.8 0.7 convolution_convert_fusion
  189.5 2.6 fusion.24
  192.1 7.1 %all-to-all-start.2 = ((bf16[64,8,2048]{2,1,0:T(8,128)(2,1)}), bf16[64,8,2048]{2,1,0:T(8,128)(2,1)S(1)}, u32[]{:S(2)}, u32[]{:S(2)}) async-start(bf16[64,8,2048]{2,1,0:T(8,128)(2,1)} %fusion.24), calls=%async_computation.2 | async-start | bytes 4194304 | tf_op jit(solution)/shard_map/all_to_all | solution.py:255
  199.2 0.8 dynamic_slice.27
  200.2 48.7 %all-to-all-done.2 = bf16[64,8,2048]{2,1,0:T(8,128)(2,1)S(1)} async-done(((bf16[64,8,2048]{2,1,0:T(8,128)(2,1)}), bf16[64,8,2048]{2,1,0:T(8,128)(2,1)S(1)}, u32[]{:S(2)}, u32[]{:S(2)}) %all-to-all-start.2) | async-done | bytes 2097184 | tf_op jit(solution)/shard_map/all_to_all | solution.py:255
  248.9 2.3 gather_fusion.1
  251.3 2.4 reshape.1527
  253.6 3.2 %multiply_reduce_fusion = f32[128,2048]{1,0:T(8,128)S(1)} fusion(f32[128,2,2048]{2,1,0:T(2,128)S(1)} %reshape.1527, f32[128,2]{1,0:T(8,128)S(1)} %copy.210), kind=kLoop, calls=%fused_computation.58 | loop fusion | flops 786432 | bytes 3146752 | tf_op jit(solution)/shard_map/reduce_sum | solution.py:268
  256.8 0.9 add_convert_fusion.1
  (228 shorter events, 25.5 us)
Async XLA Ops:
  6.5 3.1 %copy-start.3 = (bf16[1,256,2048]{2,1,0:T(8,128)(2,1)S(1)}, bf16[1,256,2048]{2,1,0:T(8,128)(2,1)}, u32[]{:S(2)}) copy-start(bf16[1,256,2048]{2,1,0:T(8,128)(2,1)} %param.33) | copy-start | bytes 3145732
  6.5 132.6 %all-gather.8.cloned.1.call-start = ((), (), s32[]{:S(2)}) async-start(), calls=%async_computation.3 | async-start | bytes 15728640 | tf_op jit(solution)/shard_map/all_gather | solution.py:22
  11.4 0.7 copy-start.8
  11.4 2.6 copy-start.7
  11.4 2.9 %copy-start.5 = (bf16[512,256]{1,0:T(8,128)(2,1)S(1)}, bf16[512,256]{1,0:T(8,128)(2,1)}, u32[]{:S(2)}) copy-start(bf16[512,256]{1,0:T(8,128)(2,1)} %param.20) | copy-start | bytes 786436
  11.4 3.3 %copy-start.2 = (bf16[512,256]{1,0:T(8,128)(2,1)S(1)}, bf16[512,256]{1,0:T(8,128)(2,1)}, u32[]{:S(2)}) copy-start(bf16[512,256]{1,0:T(8,128)(2,1)} %param.21) | copy-start | bytes 786436
  21.0 0.9 copy-start.10
  21.0 0.9 copy-start.22
  21.1 0.9 copy-start.23
  21.1 0.9 copy-start.11
  21.1 0.9 copy-start.12
  21.1 0.9 copy-start.13
  31.9 2.2 copy-start.14
  32.0 2.2 copy-start.24
  32.0 2.2 copy-start.25
  32.0 2.2 copy-start.26
  32.0 2.2 copy-start.27
  32.6 1.5 copy-start.15
  32.6 1.5 copy-start.16
  32.6 1.5 copy-start.17
  32.6 1.5 copy-start.18
  32.7 1.5 copy-start.19
  32.7 1.5 copy-start.20
  32.7 1.5 copy-start.21
  75.2 4.4 %copy-start.1 = (f32[4,128,4,64]{1,3,2,0:T(8,128)S(1)}, f32[4,128,4,64]{1,3,2,0:T(8,128)}, u32[]{:S(2)}) copy-start(f32[4,128,4,64]{1,3,2,0:T(8,128)} %custom-call.4) | copy-start | bytes 1572868
  79.5 12.5 %copy-start.6 = (bf16[512,256]{1,0:T(8,128)(2,1)S(1)}, bf16[512,256]{1,0:T(8,128)(2,1)}, u32[]{:S(2)}) copy-start(bf16[512,256]{1,0:T(8,128)(2,1)} %param.22) | copy-start | bytes 786436
  79.5 12.6 %copy-start.29 = (f32[4,64]{1,0:T(4,128)S(1)}, f32[4,64]{1,0:T(4,128)}, u32[]{:S(2)}) copy-start(f32[4,64]{1,0:T(4,128)} %param.25) | copy-start | bytes 3076
  91.6 14.1 %copy-start.4 = (bf16[128,2048]{1,0:T(8,128)(2,1)S(1)}, bf16[128,2048]{1,0:T(8,128)(2,1)}, u32[]{:S(2)}) copy-start(bf16[128,2048]{1,0:T(8,128)(2,1)} %param.18) | copy-start | bytes 1572868
  93.3 12.5 %all-to-all-start = ((bf16[4,128,256]{1,2,0:T(8,128)(2,1)}), bf16[4,128,256]{1,2,0:T(8,128)(2,1)S(1)}, u32[]{:S(2)}, u32[]{:S(2)}) async-start(bf16[4,128,256]{1,2,0:T(8,128)(2,1)} %copy_bitcast_fusion), calls=%async_computation | async-start | bytes 524288 | tf_op jit(solution)/shard_map/all_to_all | solution.py:221
  99.2 9.7 %copy-start.9 = (f32[2048]{0:T(1024)S(1)}, f32[2048]{0:T(1024)}, u32[]{:S(2)}) copy-start(f32[2048]{0:T(1024)} %param.27) | copy-start | bytes 24580
  112.4 65.4 %all-to-all-start.1 = ((bf16[64,8,2048]{2,1,0:T(8,128)(2,1)}), bf16[64,8,2048]{2,1,0:T(8,128)(2,1)S(1)}, u32[]{:S(2)}, u32[]{:S(2)}) async-start(bf16[64,8,2048]{2,1,0:T(8,128)(2,1)} %bitcast.536), calls=%async_computation.1 | async-start | bytes 4194304 | tf_op jit(solution)/shard_map/all_to_all | solution.py:241
  182.4 4.9 %copy-start = (bf16[1,1024,2048]{2,1,0:T(8,128)(2,1)S(1)}, bf16[1,1024,2048]{2,1,0:T(8,128)(2,1)}, u32[]{:S(2)}) copy-start(bf16[1,1024,2048]{2,1,0:T(8,128)(2,1)} %slice_bitcast_fusion) | copy-start | bytes 12582916
  192.1 7.1 %copy-start.28 = (f32[512,2]{0,1:T(2,128)S(1)}, f32[512,2]{0,1:T(2,128)}, u32[]{:S(2)}) copy-start(f32[512,2]{0,1:T(2,128)} %param.30) | copy-start | bytes 12292
  192.1 56.8 %all-to-all-start.2 = ((bf16[64,8,2048]{2,1,0:T(8,128)(2,1)}), bf16[64,8,2048]{2,1,0:T(8,128)(2,1)S(1)}, u32[]{:S(2)}, u32[]{:S(2)}) async-start(bf16[64,8,2048]{2,1,0:T(8,128)(2,1)} %fusion.24), calls=%async_computation.2 | async-start | bytes 4194304 | tf_op jit(solution)/shard_map/all_to_all | solution.py:255
Sparse Core Ops, SparseCore 0:
  11.6 127.5 all-gather.7
where the time goes:
time: 266 us; the launch traced here: 265 us
  waiting for transfers between devices  98.3 us (37%)
  local copies, waits for them, and re-layouts  41.8 us (16%)
  blocking collectives  39.6 us (15%)
  starting transfers between devices  26.8 us (10%)
  matrix products  25.6 us (10%)
  other arithmetic  17.8 us (7%)
  between operations  14.3 us (5%)
    all_to_all x1, waiting for transfers between devices, shards(): lax.all_to_all(returned.reshape(expert_total, capacity, model_width).asty...  48.7 us
    all_gather x3, blocking collectives, gathered_once(): both, at, found = (lax.all_gather(jnp.concatenate(lines), axis), 0, {})  39.6 us
    all_to_all x1, waiting for transfers between devices, shards(): lax.all_to_all(send_rows.reshape(expert_total, capacity, model_width), SP...  34 us
    all_to_all x1, starting transfers between devices, shards(): lax.all_to_all(send_rows.reshape(expert_total, capacity, model_width), SP...  15.7 us
    squeeze x14, local copies, waits for them, and re-layouts, entering(): subtotal = combine(subtotal, jax.tree.map(lambda part: part[k], pieces))  11 us
    all_gather x1, waiting for transfers between devices, turned_gather(): whole = lax.all_gather(both, axis, axis=0, tiled=True)  11 us
    all_to_all x1, starting transfers between devices, shards(): lax.all_to_all(returned.reshape(expert_total, capacity, model_width).asty...  7.09 us
    unnamed x68, local copies, waits for them, and re-layouts  5.49 us
  transfers between devices with their start and end apart: 4, of which 4 were waited for; matrix products, arithmetic and copies ran while one was open for 21% of the time, Pallas kernels for 0%

commit v1 on v0

v1 whole, which is shorter than its diff:
```python
import functools

import jax
import jax.numpy as jnp
from jax import lax
from jax.experimental import pallas as pl
from jax.experimental.pallas import tpu as pltpu
from jax.sharding import PartitionSpec as P

EPSILON = 1e-06
VERY_NEGATIVE = -1e30
MESH = pl.DeviceIdType.MESH
PLANE = 8
F32 = jnp.float32
BF16 = jnp.bfloat16


def dot(a, b):
    return jnp.dot(a, b, preferred_element_type=F32)


def dot_t(a, b):
    return lax.dot_general(a, b, (((1,), (1,)), ((), ())), preferred_element_type=F32)


def halves(x):
    high = x.astype(BF16)
    return high, (x - high.astype(F32)).astype(BF16)


def shifted(x, by, fill):
    lane = lax.broadcasted_iota(jnp.int32, x.shape, 1)
    return jnp.where(lane >= by, pltpu.roll(x, by, 1), fill)


def running(x, combine, fill):
    by = 1
    while by < x.shape[1]:
        x = combine(x, shifted(x, by, fill))
        by *= 2
    return x


def join(early, late):
    early_total, early_level, early_memory = early
    late_total, late_level, late_memory = late
    level = jnp.maximum(late_total + early_level, late_level)
    memory = (
        jnp.exp(late_total + early_level - level) * early_memory
        + jnp.exp(late_level - level) * late_memory
    )
    return early_total + late_total, level, memory


def packed(total, level, memory):
    row = lax.broadcasted_iota(jnp.int32, memory.shape, 0)
    return memory, jnp.where(row == 0, total, jnp.where(row == 1, level, 0.0))


def unpacked(ref, index):
    return ref[index, 8:9, :], ref[index, 9:10, :], ref[index, 0:8, :]


def put(ref, index, state):
    memory, scalars = packed(*state)
    ref[index, 0:8, :] = memory
    ref[index, 8:16, :] = scalars


def ring_peer(me, step, count):
    away = (step + 1) // 2
    sign = 2 * lax.rem(step, 2) - 1
    return lax.rem(me + sign * away + count, count)


def slots_of(routes, capacity, experts):
    tokens = routes.shape[1]
    expert = lax.broadcasted_iota(jnp.int32, (experts, tokens), 0)
    first = expert == routes[0:1, :]
    second = expert == routes[1:2, :]
    row = lax.broadcasted_iota(jnp.int32, (tokens, tokens), 0)
    column = lax.broadcasted_iota(jnp.int32, (tokens, tokens), 1)
    earlier = jnp.where(row < column, 1.0, 0.0).astype(BF16)
    ones = jnp.ones((tokens, tokens), BF16)
    first_hot = jnp.where(first, 1.0, 0.0).astype(BF16)
    second_hot = jnp.where(second, 1.0, 0.0).astype(BF16)
    first_rank = dot(first_hot, earlier)
    second_rank = dot(first_hot, ones) + dot(second_hot, earlier)
    places = []
    for hot, rank, route in ((first, first_rank, routes[0:1, :]), (second, second_rank, routes[1:2, :])):
        own = jnp.sum(jnp.where(hot, rank, 0.0), axis=0, keepdims=True)
        places.append(route * capacity + own.astype(jnp.int32))
    return places


def front_kernel(
    sp_count,
    tp_count,
    head_count,
    q_ref,
    k_ref,
    v_ref,
    og_ref,
    ig_ref,
    fg_ref,
    hgain_ref,
    wo_hbm,
    res_ref,
    ngain_ref,
    routes_ref,
    arrived_ref,
    stream_ref,
    wo_ref,
    intra_ref,
    s1_ref,
    r1_ref,
    s2_ref,
    r2_ref,
    s3_ref,
    r3_ref,
    mix_ref,
    mrecv_ref,
    send_ref,
    wo_sem,
    own_sem,
    send1,
    recv1,
    send2,
    recv2,
    send3,
    recv3,
    send4,
    recv4,
    send5,
    recv5,
):
    me = lax.axis_index("sp")
    mt = lax.axis_index("tp")
    zed = me // PLANE
    place = lax.rem(me, PLANE)
    planes = sp_count // PLANE
    length, width = q_ref.shape
    head = width // head_count
    tokens = length // tp_count

    barrier = pltpu.get_barrier_semaphore()

    def greet(step, _):
        pl.semaphore_signal(
            barrier, inc=1, device_id={"sp": ring_peer(me, step, sp_count)}, device_id_type=MESH
        )
        return 0

    lax.fori_loop(1, sp_count, greet, 0)

    def greet_tp(step, _):
        pl.semaphore_signal(
            barrier, inc=1, device_id={"tp": lax.rem(mt + step, tp_count)}, device_id_type=MESH
        )
        return 0

    lax.fori_loop(1, tp_count, greet_tp, 0)

    wo_copy = pltpu.make_async_copy(wo_hbm, wo_ref, wo_sem)
    wo_copy.start()

    small = jnp.exp(-fg_ref[...])
    series = small * (1.0 - small * (0.5 - small * (1.0 / 3.0 - 0.25 * small)))
    log_forget = -jnp.where(small < 0.01, series, jnp.log(1.0 + small))
    cum = running(log_forget, jnp.add, 0.0)
    level_in = ig_ref[...] - cum
    peak = running(level_in, jnp.maximum, VERY_NEGATIVE)
    total_col = cum[:, length - 1 : length]
    top_col = peak[:, length - 1 : length]
    weight = jnp.exp(level_in - top_col)

    lane_head = lax.broadcasted_iota(jnp.int32, (1, width), 1) // head
    masks = [lane_head == h for h in range(head_count)]

    def spread(column):
        row = jnp.zeros((1, width), F32)
        for h in range(head_count):
            row = jnp.where(masks[h], column[h : h + 1, :], row)
        return row

    total_row = spread(total_col)
    level_row = total_row + spread(top_col)

    k_turned = k_ref[...].astype(F32).T
    parts = [
        k_turned[h * head : (h + 1) * head, :] * weight[h : h + 1, :] for h in range(head_count)
    ]
    high, low = halves(jnp.concatenate(parts, axis=0))
    values = v_ref[...]
    whole = dot(high, values) + dot(low, values)
    memory = jnp.zeros((head, width), F32)
    for h in range(head_count):
        memory = jnp.where(masks[h], whole[h * head : (h + 1) * head, :], memory)
    rows = head // PLANE
    for n in range(PLANE):
        put(s1_ref, n, (total_row, level_row, memory[n * rows : (n + 1) * rows, :]))
    put(r1_ref, place, unpacked(s1_ref, place))

    pl.semaphore_wait(barrier, sp_count - 1 + tp_count - 1)

    def exchange1(step):
        peer = lax.rem(place + step, PLANE)
        return pltpu.make_async_remote_copy(
            src_ref=s1_ref.at[peer],
            dst_ref=r1_ref.at[place],
            send_sem=send1.at[peer],
            recv_sem=recv1.at[place],
            device_id={"sp": zed * PLANE + peer},
            device_id_type=MESH,
        )

    def arrival1(step):
        peer = lax.rem(place + step, PLANE)
        return pltpu.make_async_remote_copy(
            src_ref=s1_ref.at[peer],
            dst_ref=r1_ref.at[peer],
            send_sem=send1.at[peer],
            recv_sem=recv1.at[peer],
            device_id={"sp": zed * PLANE + peer},
            device_id_type=MESH,
        )

    def exchange2(step, at):
        peer = lax.rem(zed + step, planes)
        return pltpu.make_async_remote_copy(
            src_ref=s2_ref.at[0],
            dst_ref=r2_ref.at[peer if at is None else at],
            send_sem=send2.at[peer],
            recv_sem=recv2.at[peer if at is None else at],
            device_id={"sp": peer * PLANE + place},
            device_id_type=MESH,
        )

    def exchange3(step, at):
        peer = lax.rem(place + step, PLANE)
        return pltpu.make_async_remote_copy(
            src_ref=s3_ref.at[peer],
            dst_ref=r3_ref.at[peer if at is None else at],
            send_sem=send3.at[peer],
            recv_sem=recv3.at[peer if at is None else at],
            device_id={"sp": zed * PLANE + peer},
            device_id_type=MESH,
        )

    for step in range(1, PLANE):
        exchange1(step).start()

    peak_cols = jnp.concatenate([peak, jnp.zeros((8 - head_count, length), F32)], axis=0).T
    peak_wide = jnp.zeros((length, width), F32)
    for h in range(head_count):
        peak_wide = jnp.where(masks[h], peak_cols[:, h : h + 1], peak_wide)
    scale = head**-0.5
    block = 128

    def inner(t):
        span = (t + 1) * block
        rows_t = slice(t * block, span)
        query = q_ref[rows_t, :].astype(F32) * scale
        position = lax.broadcasted_iota(jnp.int32, (block, span), 0) + t * block
        source = lax.broadcasted_iota(jnp.int32, (block, span), 1)
        causal = source <= position
        found = jnp.zeros((block, width), F32)
        for h in range(head_count):
            mine = jnp.where(masks[h], query, 0.0).astype(BF16)
            scores = dot_t(mine, k_ref[0:span, :])
            gap = level_in[h : h + 1, 0:span] - peak_cols[rows_t, h : h + 1]
            pairs = scores * jnp.exp(jnp.where(causal, gap, VERY_NEGATIVE))
            pairs_high, pairs_low = halves(pairs)
            part = dot(pairs_high, v_ref[0:span, :]) + dot(pairs_low, v_ref[0:span, :])
            found = jnp.where(masks[h], part, found)
        intra_ref[rows_t, :] = found

    inner(0)
    inner(1)

    for step in range(1, PLANE):
        arrival1(step).wait()
    identity = (
        jnp.zeros((1, width), F32),
        jnp.full((1, width), VERY_NEGATIVE, F32),
        jnp.zeros((rows, width), F32),
    )
    prior = [identity]
    for n in range(PLANE):
        prior.append(join(prior[-1], unpacked(r1_ref, n)))
    put(s2_ref, 0, prior[-1])
    put(r2_ref, zed, prior[-1])
    for step in range(1, planes):
        exchange2(step, zed).start()

    inner(2)

    for step in range(1, planes):
        exchange2(step, None).wait()
    entering = identity
    for n in range(planes):
        later = join(entering, unpacked(r2_ref, n))
        entering = tuple(jnp.where(n < zed, new, old) for new, old in zip(later, entering))
    for n in range(PLANE):
        put(s3_ref, n, join(entering, prior[n]))
    put(r3_ref, place, unpacked(s3_ref, place))
    for step in range(1, PLANE):
        exchange3(step, place).start()

    inner(3)

    for step in range(1, PLANE):
        exchange3(step, None).wait()
    prior_total = r3_ref[0, 8:9, :]
    prior_level = r3_ref[0, 9:10, :]
    start_level = jnp.maximum(prior_level, prior_total)
    opening = jnp.exp(prior_level - start_level)
    began = jnp.concatenate([r3_ref[n, 0:8, :] for n in range(PLANE)], axis=0) * opening
    blocks = jnp.concatenate([jnp.where(masks[h], began, 0.0) for h in range(head_count)], axis=0)
    block_high, block_low = halves(blocks)
    queries = (q_ref[...].astype(F32) * scale).astype(BF16)
    carried = dot(queries, block_high) + dot(queries, block_low)
    level = jnp.maximum(peak_wide, start_level)
    cell = jnp.exp(peak_wide - level) * intra_ref[...] + jnp.exp(start_level - level) * carried
    row_head = lax.broadcasted_iota(jnp.int32, (width, width), 0) // head
    column_head = lax.broadcasted_iota(jnp.int32, (width, width), 1) // head
    averaging = jnp.where(row_head == column_head, 1.0 / head, 0.0).astype(BF16)
    square_high, square_low = halves(cell * cell)
    mean = dot(square_high, averaging) + dot(square_low, averaging)
    gate = 1.0 / (1.0 + jnp.exp(-og_ref[...].astype(F32)))
    mixed = (gate * (cell * lax.rsqrt(mean + EPSILON) * hgain_ref[...])).astype(BF16)
    for n in range(tp_count):
        mix_ref[n] = mixed[n * tokens : (n + 1) * tokens, :]

    def exchange4(step, at):
        peer = lax.rem(mt + step, tp_count)
        return pltpu.make_async_remote_copy(
            src_ref=mix_ref.at[peer],
            dst_ref=mrecv_ref.at[peer if at is None else at],
            send_sem=send4.at[peer],
            recv_sem=recv4.at[peer if at is None else at],
            device_id={"tp": peer},
            device_id_type=MESH,
        )

    for step in range(1, tp_count):
        exchange4(step, mt).start()
    mrecv_ref[mt] = mix_ref[mt]

    routes = routes_ref[:, pl.ds(pl.multiple_of(mt * tokens, tokens), tokens)]
    capacity = send_ref.shape[1]
    slots = sp_count * capacity
    first, second = slots_of(routes, capacity, sp_count)
    slot = lax.broadcasted_iota(jnp.int32, (slots, tokens), 0)
    select = jnp.where((slot == first) | (slot == second), 1.0, 0.0).astype(BF16)

    wo_copy.wait()
    for step in range(1, tp_count):
        exchange4(step, None).wait()
    gathered = jnp.concatenate([mrecv_ref[n] for n in range(tp_count)], axis=1)
    model = wo_ref.shape[1]
    piece = 512
    squares = jnp.zeros((tokens, 1), F32)
    for n in range(model // piece):
        cols = slice(n * piece, (n + 1) * piece)
        projected = dot(gathered, wo_ref[:, cols])
        stream = (res_ref[:, cols].astype(F32) + projected).astype(BF16)
        stream_ref[:, cols] = stream
        stream = stream.astype(F32)
        squares = squares + jnp.sum(stream * stream, axis=1, keepdims=True)
    inverse = lax.rsqrt(squares * (1.0 / model) + EPSILON)
    for n in range(model // piece):
        cols = slice(n * piece, (n + 1) * piece)
        normed = (stream_ref[:, cols].astype(F32) * inverse * ngain_ref[:, cols]).astype(BF16)
        chosen = dot(select, normed).reshape(sp_count, capacity, piece)
        send_ref[:, :, cols] = chosen.astype(BF16)

    own_copy = pltpu.make_async_copy(send_ref.at[me], arrived_ref.at[me], own_sem)
    own_copy.start()

    def dispatch(step, at):
        peer = ring_peer(me, step, sp_count)
        return pltpu.make_async_remote_copy(
            src_ref=send_ref.at[peer],
            dst_ref=arrived_ref.at[peer if at is None else at],
            send_sem=send5.at[peer],
            recv_sem=recv5.at[peer if at is None else at],
            device_id={"sp": peer},
            device_id_type=MESH,
        )

    def go(step, _):
        dispatch(step, me).start()
        return 0

    def done(step, _):
        dispatch(step, None).wait()
        return 0

    lax.fori_loop(1, sp_count, go, 0)
    lax.fori_loop(1, sp_count, done, 0)
    own_copy.wait()


def hidden_kernel(rows_ref, gate_ref, up_ref, hidden_ref):
    rows = rows_ref[...]
    gate = dot(rows, gate_ref[0])
    up = dot(rows, up_ref[0])
    hidden_ref[...] = (gate / (1.0 + jnp.exp(-gate)) * up).astype(BF16)


def back_kernel(
    sp_count,
    tp_count,
    hidden_ref,
    down_ref,
    stream_ref,
    routes_ref,
    group_ref,
    scores_ref,
    out_ref,
    send_ref,
    answer_ref,
    send_sem,
    recv_sem,
):
    me = lax.axis_index("sp")
    mt = lax.axis_index("tp")
    barrier = pltpu.get_barrier_semaphore()

    def greet(step, _):
        pl.semaphore_signal(
            barrier, inc=1, device_id={"sp": ring_peer(me, step, sp_count)}, device_id_type=MESH
        )
        return 0

    lax.fori_loop(1, sp_count, greet, 0)
    capacity = send_ref.shape[1]
    model = send_ref.shape[2]
    slots = sp_count * capacity
    tokens = stream_ref.shape[0]
    piece = 512
    hidden = hidden_ref[...]
    for n in range(model // piece):
        cols = slice(n * piece, (n + 1) * piece)
        result = dot(hidden, down_ref[:, cols]).reshape(sp_count, capacity, piece)
        send_ref[:, :, cols] = result.astype(BF16)
    answer_ref[me] = send_ref[me]
    pl.semaphore_wait(barrier, sp_count - 1)

    def give(step, at):
        peer = ring_peer(me, step, sp_count)
        return pltpu.make_async_remote_copy(
            src_ref=send_ref.at[peer],
            dst_ref=answer_ref.at[peer if at is None else at],
            send_sem=send_sem.at[peer],
            recv_sem=recv_sem.at[peer if at is None else at],
            device_id={"sp": peer},
            device_id_type=MESH,
        )

    def go(step, _):
        give(step, me).start()
        return 0

    def done(step, _):
        give(step, None).wait()
        return 0

    lax.fori_loop(1, sp_count, go, 0)

    own = pl.ds(pl.multiple_of(mt * tokens, tokens), tokens)
    first, second = slots_of(routes_ref[:, own], capacity, sp_count)
    scores = scores_ref[:, own]
    most = jnp.maximum(scores[0:1, :], scores[1:2, :])
    first_exp = jnp.exp(scores[0:1, :] - most)
    second_exp = jnp.exp(scores[1:2, :] - most)
    share = group_ref[:, own] / (first_exp + second_exp)
    slot = lax.broadcasted_iota(jnp.int32, (slots, tokens), 0)
    weights = jnp.where(slot == first, share * first_exp, 0.0)
    weights = jnp.where(slot == second, share * second_exp, weights).T
    weights_high, weights_low = halves(weights)

    lax.fori_loop(1, sp_count, done, 0)
    for n in range(model // piece):
        cols = slice(n * piece, (n + 1) * piece)
        answers = answer_ref[:, :, cols].astype(F32).reshape(slots, piece).astype(BF16)
        mix = dot(weights_high, answers) + dot(weights_low, answers)
        out_ref[:, cols] = (stream_ref[:, cols].astype(F32) + mix).astype(BF16)


def shards(
    residual,
    queries,
    key_vectors,
    value_vectors,
    output_gate,
    input_gate,
    forget_gate,
    head_gain,
    output_weight,
    norm_gain,
    route_experts,
    group_weight,
    expert_scores,
    gate_weight,
    up_weight,
    down_weight,
):
    sp_count = lax.axis_size("sp")
    tp_count = lax.axis_size("tp")
    length, width = queries.shape
    head_count = input_gate.shape[1]
    tokens, model = residual.shape
    capacity = 4 * tokens // sp_count
    hidden_part = gate_weight.shape[2]
    hidden_all = hidden_part * tp_count

    gates = lax.all_gather(gate_weight[0], "tp", axis=0, tiled=False)
    ups = lax.all_gather(up_weight[0], "tp", axis=0, tiled=False)
    downs = lax.all_gather(down_weight[0], "tp", axis=0, tiled=True)

    routes = route_experts.T
    vmem = pl.BlockSpec(memory_space=pltpu.VMEM)
    hbm = pl.BlockSpec(memory_space=pl.ANY)
    dma = pltpu.SemaphoreType.DMA
    planes = sp_count // PLANE
    arrived, stream = pl.pallas_call(
        functools.partial(front_kernel, sp_count, tp_count, head_count),
        out_shape=(
            jax.ShapeDtypeStruct((sp_count, capacity, model), BF16),
            jax.ShapeDtypeStruct((tokens, model), BF16),
        ),
        in_specs=[vmem] * 7 + [hbm] + [vmem] * 3,
        out_specs=(hbm, vmem),
        scratch_shapes=[
            pltpu.VMEM(output_weight.shape, BF16),
            pltpu.VMEM((length, width), F32),
            pltpu.VMEM((PLANE, 16, width), F32),
            pltpu.VMEM((PLANE, 16, width), F32),
            pltpu.VMEM((1, 16, width), F32),
            pltpu.VMEM((planes, 16, width), F32),
            pltpu.VMEM((PLANE, 16, width), F32),
            pltpu.VMEM((PLANE, 16, width), F32),
            pltpu.VMEM((tp_count, tokens, width), BF16),
            pltpu.VMEM((tp_count, tokens, width), BF16),
            pltpu.VMEM((sp_count, capacity, model), BF16),
            dma,
            dma,
            dma((PLANE,)),
            dma((PLANE,)),
            dma((planes,)),
            dma((planes,)),
            dma((PLANE,)),
            dma((PLANE,)),
            dma((tp_count,)),
            dma((tp_count,)),
            dma((sp_count,)),
            dma((sp_count,)),
        ],
        compiler_params=pltpu.CompilerParams(
            collective_id=0, has_side_effects=True, vmem_limit_bytes=40 * 2**20
        ),
        cost_estimate=pl.CostEstimate(
            flops=60_000_000_000, bytes_accessed=10_000_000, transcendentals=0
        ),
    )(
        queries,
        key_vectors,
        value_vectors,
        output_gate,
        input_gate.T,
        forget_gate.T,
        head_gain.reshape(1, width),
        output_weight,
        residual,
        norm_gain.reshape(1, model),
        routes,
    )

    slots = sp_count * capacity
    hidden = pl.pallas_call(
        hidden_kernel,
        grid=(tp_count,),
        out_shape=jax.ShapeDtypeStruct((slots, hidden_all), BF16),
        in_specs=[
            pl.BlockSpec((slots, model), lambda n: (0, 0)),
            pl.BlockSpec((1, model, hidden_part), lambda n: (n, 0, 0)),
            pl.BlockSpec((1, model, hidden_part), lambda n: (n, 0, 0)),
        ],
        out_specs=pl.BlockSpec((slots, hidden_part), lambda n: (0, n)),
        compiler_params=pltpu.CompilerParams(vmem_limit_bytes=40 * 2**20),
        cost_estimate=pl.CostEstimate(
            flops=4 * slots * model * hidden_all,
            bytes_accessed=4 * model * hidden_all,
            transcendentals=slots * hidden_all,
        ),
    )(arrived.reshape(slots, model), gates, ups)

    return pl.pallas_call(
        functools.partial(back_kernel, sp_count, tp_count),
        out_shape=jax.ShapeDtypeStruct((tokens, model), BF16),
        in_specs=[vmem] * 6,
        out_specs=vmem,
        scratch_shapes=[
            pltpu.VMEM((sp_count, capacity, model), BF16),
            pltpu.VMEM((sp_count, capacity, model), BF16),
            dma((sp_count,)),
            dma((sp_count,)),
        ],
        compiler_params=pltpu.CompilerParams(
            collective_id=1, has_side_effects=True, vmem_limit_bytes=40 * 2**20
        ),
        cost_estimate=pl.CostEstimate(
            flops=60_000_000_000, bytes_accessed=10_000_000, transcendentals=0
        ),
    )(hidden, downs, stream, routes, group_weight.reshape(1, length), expert_scores.T)


def solution(mesh):
    both = ("sp", "tp")
    return jax.shard_map(
        shards,
        mesh=mesh,
        in_specs=(
            P(both, None),
            P("sp", "tp"),
            P("sp", "tp"),
            P("sp", "tp"),
            P("sp", "tp"),
            P("sp", "tp"),
            P("sp", "tp"),
            P("tp", None),
            P(),
            P(),
            P("sp", None),
            P("sp"),
            P("sp", None),
            P("sp", None, "tp"),
            P("sp", None, "tp"),
            P("sp", "tp", None),
        ),
        out_specs=P(both, None),
        check_vma=False,
    )
```

time: 266 us -> 241 us (0.906)
  Pallas kernels: 0 us -> 150 us
  waiting for transfers between devices: 98.3 us -> 57.9 us
  blocking collectives: 39.6 us -> 0 us
  starting transfers between devices: 26.8 us -> 0.08 us
  matrix products: 25.6 us -> 0 us
  local copies, waits for them, and re-layouts: 41.8 us -> 19.8 us
  other arithmetic: 17.8 us -> 0 us
    pallas_call x0 -> x3, Pallas kernels: none -> 150 us  [the longest x1 86.9 us: shards(): pl.pallas_call(functools.partial(front_kernel, sp_count, tp_count, head_c...]
    all_to_all x3 -> x0, waiting for transfers between devices: 87.3 us -> none  [the longest x1 48.7 us: shards(): lax.all_to_all(returned.reshape(expert_total, capacity, model_width).asty...]
    all_gather x1 -> x3, waiting for transfers between devices: 11 us -> 55.8 us  [the longest x1 43.3 us: shards(): downs = lax.all_gather(down_weight[0], 'tp', axis=0, tiled=True)]
    all_gather x3 -> x0, blocking collectives: 39.6 us -> none  [gathered_once(): both, at, found = (lax.all_gather(jnp.concatenate(lines), axis), 0, {})]
    all_to_all x3 -> x0, starting transfers between devices: 26.8 us -> none  [the longest x1 15.7 us: shards(): lax.all_to_all(send_rows.reshape(expert_total, capacity, model_width), SP...]
    dot_general x24 -> x0, matrix products: 25.6 us -> none  [the longest x1 4.87 us: expert_whole(): jnp.dot(chosen_rows, whole_up[0], preferred_element_type=jnp.float32)]
    unnamed x68 -> x37, local copies, waits for them, and re-layouts: 5.49 us -> 19 us
    squeeze x14 -> x0, local copies, waits for them, and re-layouts: 11 us -> none  [entering(): subtotal = combine(subtotal, jax.tree.map(lambda part: part[k], pieces))]
  transfers between devices with their start and end apart: 4 -> 3, of which waited for: 4 -> 2; matrix products, arithmetic and copies ran while one was open for 21% -> 0% of each run, Pallas kernels for 0% -> 38%
where the time goes in v1:
time: 241 us
  Pallas kernels  150 us (62%)
  waiting for transfers between devices  57.9 us (24%)
  local copies, waits for them, and re-layouts  19.8 us (8%)
  between operations  13.2 us (5%)
    pallas_call x1, Pallas kernels, shards(): pl.pallas_call(functools.partial(front_kernel, sp_count, tp_count, head_c...  86.9 us
    pallas_call x1, Pallas kernels, shards(): pl.pallas_call(functools.partial(back_kernel, sp_count, tp_count), out_sh...  57.4 us
    all_gather x1, waiting for transfers between devices, shards(): downs = lax.all_gather(down_weight[0], 'tp', axis=0, tiled=True)  43.3 us
    unnamed x37, local copies, waits for them, and re-layouts  19 us
    all_gather x1, waiting for transfers between devices, shards(): ups = lax.all_gather(up_weight[0], 'tp', axis=0, tiled=False)  12.5 us
    pallas_call x1, Pallas kernels, shards(): pl.pallas_call(hidden_kernel, grid=(tp_count,), out_shape=jax.ShapeDtypeS...  5.28 us
  transfers between devices with their start and end apart: 3, of which 2 were waited for; matrix products, arithmetic and copies ran while one was open for 0% of the time, Pallas kernels for 38%

profile of v1, /device:TPU:1, one launch (start us, length us, event | category | flops | bytes accessed | tf_op | source)
XLA Modules:
  0.0 240.5 jit_solution(1179944343835729981)
XLA Ops:
  6.5 0.0 all-gather.5.cloned.1.call-start
  6.5 0.7 all-gather.5.cloned.1.call-update
  7.3 0.0 all-gather.7.cloned.1.call-start
  7.3 0.7 all-gather.7.cloned.1.call-update
  8.0 0.0 all-gather.9.cloned.1.call-start
  8.1 0.7 all-gather.9.cloned.1.call-update
  8.7 0.8 reshape.12.hgain_ref
  9.5 0.0 copy-start
  9.5 2.2 copy-done
  11.7 0.0 copy-start.4
  11.7 1.0 copy-done.4
  12.7 0.0 copy-start.5
  12.7 0.9 copy-done.5
  13.7 0.0 copy-start.6
  13.7 0.9 copy-done.6
  14.6 0.0 copy-start.7
  14.6 0.9 copy-done.7
  15.6 0.0 copy-start.8
  15.6 0.9 copy-done.8
  16.5 0.0 copy-start.9
  16.5 0.7 copy-done.9
  17.2 0.0 copy-start.10
  17.2 0.7 copy-done.10
  17.9 0.0 copy-start.11
  17.9 0.7 copy-done.11
  18.6 0.0 copy-start.12
  18.6 0.7 copy-done.12
  19.3 86.9 %shard_map.154 = (bf16[64,8,2048]{2,1,0:T(8,128)(2,1)S(1)}, bf16[128,2048]{1,0:T(8,128)(2,1)S(1)}) custom-call(bf16[512,256]{1,0:T(8,128)(2,1)S(1)} %copy-done.5, bf16[512,256]{1,0:T(8,128)(2,1)S(1)} %copy-done.6, bf16[512,256]{1,0:T(8,128)(2,1)S(1)} %copy-done.7, bf16[512,256]{1,0:T(8,128)(2,1)S(1)} %copy-done.8, f32[4,512]{1,0:T(4,128)S(1)} %bitcast.9, ...), custom_call_target="tpu_custom_call" | custom-call | flops 60000002048 | bytes 10000000 | tf_op jit(solution)/shard_map/pallas_call | solution.py:528
  106.2 0.0 copy-start.16
  106.2 0.8 copy-done.16
  107.0 0.0 all-gather.5.cloned.1.call-done.gate_ref
  107.0 12.5 %all-gather.7.cloned.1.call-done.up_ref = bf16[4,2048,256]{2,1,0:T(8,128)(2,1)} async-done(((bf16[1,2048,256]{2,1,0:T(8,128)(2,1)}), bf16[4,2048,256]{2,1,0:T(8,128)(2,1)}) %all-gather.7.cloned.1.call-update) | async-done | bytes 4194320 | tf_op jit(solution)/shard_map/all_gather | solution.py:520
  119.6 0.0 copy-start.1
  119.6 2.2 copy-done.1
  121.7 2.2 copy-done.2
  123.9 0.0 copy-start.13
  123.9 0.0 copy-start.14
  123.9 0.0 copy-start.15
  123.9 5.3 %shard_map.155.hidden_ref = bf16[512,1024]{1,0:T(8,128)(2,1)S(1)} custom-call(bf16[512,2048]{1,0:T(8,128)(2,1)S(1)} %bitcast.16, bf16[4,2048,256]{2,1,0:T(8,128)(2,1)S(1)} %copy-done.1, bf16[4,2048,256]{2,1,0:T(8,128)(2,1)S(1)} %copy-done.2), custom_call_target="tpu_custom_call" | custom-call | flops 4294967296 | bytes 8388608 | tf_op jit(solution)/shard_map/pallas_call | solution.py:582
  129.2 43.3 %all-gather.9.cloned.1.call-done = bf16[1,1024,2048]{2,1,0:T(8,128)(2,1)} async-done(((bf16[1,256,2048]{2,1,0:T(8,128)(2,1)}), bf16[1,1024,2048]{2,1,0:T(8,128)(2,1)}) %all-gather.9.cloned.1.call-update) | async-done | bytes 4194320 | tf_op jit(solution)/shard_map/all_gather | solution.py:521
  172.5 0.0 copy-done.13
  172.5 0.0 copy-done.14
  172.5 0.0 copy-done.15
  172.5 0.0 copy-start.3
  172.5 2.2 copy-done.3
  174.7 1.0 copy-done.17
  175.8 57.4 %shard_map.156 = bf16[128,2048]{1,0:T(8,128)(2,1)S(1)} custom-call(bf16[512,1024]{1,0:T(8,128)(2,1)S(1)} %shard_map.155.hidden_ref, bf16[1024,2048]{1,0:T(8,128)(2,1)S(1)} %bitcast.8, bf16[128,2048]{1,0:T(8,128)(2,1)S(1)} %copy-done.17, s32[2,512]{1,0:T(2,128)S(1)} %bitcast.13, f32[1,512]{1,0:T(1,128)S(1)} %bitcast.15, f32[2,512]{1,0:T(2,128)S(1)} %bitcast.14), custom_call_target="tpu_custom_call" | custom-call | flops 60000002048 | bytes 10000000 | tf_op jit(solution)/shard_map/pallas_call | solution.py:600
  233.2 0.8 copy.18
  (2 shorter events, 0.0 us)
Async XLA Ops:
  6.5 100.5 %all-gather.5.cloned.1.call-start = ((), (), s32[]{:S(2)}) async-start(), calls=%async_computation | async-start | bytes 5242880 | tf_op jit(solution)/shard_map/all_gather | solution.py:519
  7.3 112.3 %all-gather.7.cloned.1.call-start = ((), (), s32[]{:S(2)}) async-start(), calls=%async_computation.1 | async-start | bytes 5242880 | tf_op jit(solution)/shard_map/all_gather | solution.py:520
  8.0 164.5 %all-gather.9.cloned.1.call-start = ((), (), s32[]{:S(2)}) async-start(), calls=%async_computation.2 | async-start | bytes 5242880 | tf_op jit(solution)/shard_map/all_gather | solution.py:521
  9.5 2.2 copy-start
  11.7 1.0 copy-start.4
  12.7 0.9 copy-start.5
  13.7 0.9 copy-start.6
  14.6 0.9 copy-start.7
  15.6 0.9 copy-start.8
  16.5 0.7 copy-start.9
  17.2 0.7 copy-start.10
  17.9 0.7 copy-start.11
  18.6 0.7 copy-start.12
  106.2 0.8 copy-start.16
  119.6 2.2 copy-start.1
  121.7 2.2 copy-start.2
  123.9 48.6 %copy-start.13 = (s32[512,2]{0,1:T(2,128)S(1)}, s32[512,2]{0,1:T(2,128)}, u32[]{:S(2)}) copy-start(s32[512,2]{0,1:T(2,128)} %param.26) | copy-start | bytes 12292
  123.9 48.6 %copy-start.14 = (f32[512,2]{0,1:T(2,128)S(1)}, f32[512,2]{0,1:T(2,128)}, u32[]{:S(2)}) copy-start(f32[512,2]{0,1:T(2,128)} %param.28) | copy-start | bytes 12292
  123.9 48.6 %copy-start.15 = (f32[512]{0:T(512)S(1)}, f32[512]{0:T(512)}, u32[]{:S(2)}) copy-start(f32[512]{0:T(512)} %param.27) | copy-start | bytes 6148
  172.5 2.2 copy-start.3
  174.7 1.0 copy-start.17
Sparse Core Ops, SparseCore 0:
  9.1 57.2 all-gather.4
  68.2 51.3 all-gather.6
  121.4 51.1 all-gather.8

commit v2 on v1

--- a/solution.py
+++ b/solution.py
@@ -93,47 +93,137 @@
     return places
 
 
-def front_kernel(
-    sp_count,
-    tp_count,
-    head_count,
-    q_ref,
-    k_ref,
-    v_ref,
-    og_ref,
-    ig_ref,
-    fg_ref,
-    hgain_ref,
-    wo_hbm,
-    res_ref,
-    ngain_ref,
-    routes_ref,
-    arrived_ref,
-    stream_ref,
-    wo_ref,
-    intra_ref,
-    s1_ref,
-    r1_ref,
-    s2_ref,
-    r2_ref,
-    s3_ref,
-    r3_ref,
-    mix_ref,
-    mrecv_ref,
-    send_ref,
-    wo_sem,
-    own_sem,
-    send1,
-    recv1,
-    send2,
-    recv2,
-    send3,
-    recv3,
-    send4,
-    recv4,
-    send5,
-    recv5,
-):
+class Ring:
+    def __init__(self, ref, item, me, count, sends, arrivals):
+        self.ref, self.item, self.me, self.count = ref, item, me, count
+        self.sends, self.arrivals = sends, arrivals
+        self.half = ref.shape[1] // 2
+
+    def copy(self, kind):
+        right = lax.rem(self.me + 1, self.count)
+        left = lax.rem(self.me + self.count - 1, self.count)
+        first, last = pl.ds(0, self.half), pl.ds(self.half, self.half)
+        source, target = (
+            (self.ref.at[self.me], right),
+            (self.ref.at[self.me], left),
+            (self.ref.at[left, first], right),
+            (self.ref.at[right, last], left),
+        )[kind]
+        return pltpu.make_async_remote_copy(
+            src_ref=source,
+            dst_ref=source,
+            send_sem=self.sends.at[self.item, kind],
+            recv_sem=self.arrivals.at[self.item, kind],
+            device_id={"tp": target},
+            device_id_type=MESH,
+        )
+
+    def arrival(self, kind):
+        right = lax.rem(self.me + 1, self.count)
+        left = lax.rem(self.me + self.count - 1, self.count)
+        across = lax.rem(self.me + 2, self.count)
+        first, last = pl.ds(0, self.half), pl.ds(self.half, self.half)
+        source, landed = (
+            (self.ref.at[self.me], self.ref.at[left]),
+            (self.ref.at[self.me], self.ref.at[right]),
+            (self.ref.at[left, first], self.ref.at[across, first]),
+            (self.ref.at[right, last], self.ref.at[across, last]),
+        )[kind]
+        return pltpu.make_async_remote_copy(
+            src_ref=source,
+            dst_ref=landed,
+            send_sem=self.sends.at[self.item, kind],
+            recv_sem=self.arrivals.at[self.item, kind],
+            device_id={"tp": right},
+            device_id_type=MESH,
+        )
+
+    def start(self):
+        self.copy(0).start()
+        self.copy(1).start()
+
+    def forward(self):
+        self.arrival(0).wait_recv()
+        self.copy(2).start()
+        self.arrival(1).wait_recv()
+        self.copy(3).start()
+
+    def complete(self):
+        self.arrival(2).wait_recv()
+        self.arrival(3).wait_recv()
+
+    def sent(self):
+        for kind in range(4):
+            self.copy(kind).wait_send()
+
+
+def layer_kernel(sp_count, tp_count, head_count, *refs):
+    (
+        q_hbm,
+        k_hbm,
+        v_hbm,
+        og_hbm,
+        ig_hbm,
+        fg_hbm,
+        hgain_hbm,
+        wo_hbm,
+        res_hbm,
+        ngain_hbm,
+        routes_hbm,
+        group_hbm,
+        scores_hbm,
+        gate_hbm,
+        up_hbm,
+        down_hbm,
+        out_ref,
+        q_ref,
+        k_ref,
+        v_ref,
+        og_ref,
+        ig_ref,
+        fg_ref,
+        hgain_ref,
+        wo_ref,
+        res_ref,
+        ngain_ref,
+        routes_ref,
+        group_ref,
+        scores_ref,
+        gate_ref,
+        up_ref,
+        down_a_ref,
+        down_b_ref,
+        intra_ref,
+        s1_ref,
+        r1_ref,
+        s2_ref,
+        r2_ref,
+        s3_ref,
+        r3_ref,
+        mix_ref,
+        mrecv_ref,
+        stream_ref,
+        send_ref,
+        arrived_ref,
+        hidden_ref,
+        back_ref,
+        answer_ref,
+        load_sem,
+        send1,
+        recv1,
+        send2,
+        recv2,
+        send3,
+        recv3,
+        send4,
+        recv4,
+        send5,
+        recv5,
+        send6,
+        recv6,
+        ring_send,
+        ring_recv,
+    ) = refs
     me = lax.axis_index("sp")
     mt = lax.axis_index("tp")
     zed = me // PLANE
@@ -142,6 +232,36 @@
     length, width = q_ref.shape
     head = width // head_count
     tokens = length // tp_count
+    capacity = send_ref.shape[1]
+    model = send_ref.shape[2]
+    slots = sp_count * capacity
+    column_half = model // 2
+
+    loads = [
+        (fg_hbm, fg_ref),
+        (ig_hbm, ig_ref),
+        (k_hbm, k_ref),
+        (v_hbm, v_ref),
+        (q_hbm, q_ref),
+        (gate_hbm.at[0], gate_ref.at[mt]),
+        (og_hbm, og_ref),
+        (hgain_hbm, hgain_ref),
+        (ngain_hbm, ngain_ref),
+        (routes_hbm, routes_ref),
+        (group_hbm, group_ref),
+        (scores_hbm, scores_ref),
+        (res_hbm, res_ref),
+        (up_hbm.at[0], up_ref.at[mt]),
+        (wo_hbm, wo_ref),
+        (down_hbm.at[0, :, pl.ds(0, column_half)], down_a_ref.at[mt]),
+        (down_hbm.at[0, :, pl.ds(column_half, column_half)], down_b_ref.at[mt]),
+    ]
+    loads = [
+        pltpu.make_async_copy(source, target, load_sem.at[n])
+        for n, (source, target) in enumerate(loads)
+    ]
+    for load in loads:
+        load.start()
 
     barrier = pltpu.get_barrier_semaphore()
 
@@ -161,8 +281,12 @@
 
     lax.fori_loop(1, tp_count, greet_tp, 0)
 
-    wo_copy = pltpu.make_async_copy(wo_hbm, wo_ref, wo_sem)
-    wo_copy.start()
+    gate_ring, up_ring, down_a_ring, down_b_ring = [
+        Ring(ref, item, mt, tp_count, ring_send, ring_recv)
+        for item, ref in enumerate((gate_ref, up_ref, down_a_ref, down_b_ref))
+    ]
+    for load in loads[:6]:
+        load.wait()
 
     small = jnp.exp(-fg_ref[...])
     series = small * (1.0 - small * (0.5 - small * (1.0 / 3.0 - 0.25 * small)))
@@ -249,6 +373,7 @@
 
     for step in range(1, PLANE):
         exchange1(step).start()
+    gate_ring.start()
 
     peak_cols = jnp.concatenate([peak, jnp.zeros((8 - head_count, length), F32)], axis=0).T
     peak_wide = jnp.zeros((length, width), F32)
@@ -327,8 +452,11 @@
     averaging = jnp.where(row_head == column_head, 1.0 / head, 0.0).astype(BF16)
     square_high, square_low = halves(cell * cell)
     mean = dot(square_high, averaging) + dot(square_low, averaging)
+    for load in loads[6:]:
+        load.wait()
+    gain = jnp.concatenate([hgain_ref[h : h + 1, :] for h in range(head_count)], axis=1)
     gate = 1.0 / (1.0 + jnp.exp(-og_ref[...].astype(F32)))
-    mixed = (gate * (cell * lax.rsqrt(mean + EPSILON) * hgain_ref[...])).astype(BF16)
+    mixed = (gate * (cell * lax.rsqrt(mean + EPSILON) * gain)).astype(BF16)
     for n in range(tp_count):
         mix_ref[n] = mixed[n * tokens : (n + 1) * tokens, :]
 
@@ -345,20 +473,17 @@
 
     for step in range(1, tp_count):
         exchange4(step, mt).start()
+    up_ring.start()
     mrecv_ref[mt] = mix_ref[mt]
 
     routes = routes_ref[:, pl.ds(pl.multiple_of(mt * tokens, tokens), tokens)]
-    capacity = send_ref.shape[1]
-    slots = sp_count * capacity
     first, second = slots_of(routes, capacity, sp_count)
     slot = lax.broadcasted_iota(jnp.int32, (slots, tokens), 0)
     select = jnp.where((slot == first) | (slot == second), 1.0, 0.0).astype(BF16)
 
-    wo_copy.wait()
     for step in range(1, tp_count):
         exchange4(step, None).wait()
     gathered = jnp.concatenate([mrecv_ref[n] for n in range(tp_count)], axis=1)
-    model = wo_ref.shape[1]
     piece = 512
     squares = jnp.zeros((tokens, 1), F32)
     for n in range(model // piece):
@@ -375,8 +500,7 @@
         chosen = dot(select, normed).reshape(sp_count, capacity, piece)
         send_ref[:, :, cols] = chosen.astype(BF16)
 
-    own_copy = pltpu.make_async_copy(send_ref.at[me], arrived_ref.at[me], own_sem)
-    own_copy.start()
+    arrived_ref[me] = send_ref[me]
 
     def dispatch(step, at):
         peer = ring_peer(me, step, sp_count)
@@ -398,95 +522,88 @@
         return 0
 
     lax.fori_loop(1, sp_count, go, 0)
-    lax.fori_loop(1, sp_count, done, 0)
-    own_copy.wait()
-
-
-def hidden_kernel(rows_ref, gate_ref, up_ref, hidden_ref):
-    rows = rows_ref[...]
-    gate = dot(rows, gate_ref[0])
-    up = dot(rows, up_ref[0])
-    hidden_ref[...] = (gate / (1.0 + jnp.exp(-gate)) * up).astype(BF16)
-
-
-def back_kernel(
-    sp_count,
-    tp_count,
-    hidden_ref,
-    down_ref,
-    stream_ref,
-    routes_ref,
-    group_ref,
-    scores_ref,
-    out_ref,
-    send_ref,
-    answer_ref,
-    send_sem,
-    recv_sem,
-):
-    me = lax.axis_index("sp")
-    mt = lax.axis_index("tp")
-    barrier = pltpu.get_barrier_semaphore()
-
-    def greet(step, _):
-        pl.semaphore_signal(
-            barrier, inc=1, device_id={"sp": ring_peer(me, step, sp_count)}, device_id_type=MESH
-        )
-        return 0
-
-    lax.fori_loop(1, sp_count, greet, 0)
-    capacity = send_ref.shape[1]
-    model = send_ref.shape[2]
-    slots = sp_count * capacity
-    tokens = stream_ref.shape[0]
-    piece = 512
-    hidden = hidden_ref[...]
-    for n in range(model // piece):
-        cols = slice(n * piece, (n + 1) * piece)
-        result = dot(hidden, down_ref[:, cols]).reshape(sp_count, capacity, piece)
-        send_ref[:, :, cols] = result.astype(BF16)
-    answer_ref[me] = send_ref[me]
-    pl.semaphore_wait(barrier, sp_count - 1)
-
-    def give(step, at):
-        peer = ring_peer(me, step, sp_count)
-        return pltpu.make_async_remote_copy(
-            src_ref=send_ref.at[peer],
-            dst_ref=answer_ref.at[peer if at is None else at],
-            send_sem=send_sem.at[peer],
-            recv_sem=recv_sem.at[peer if at is None else at],
-            device_id={"sp": peer},
-            device_id_type=MESH,
-        )
-
-    def go(step, _):
-        give(step, me).start()
-        return 0
-
-    def done(step, _):
-        give(step, None).wait()
-        return 0
-
-    lax.fori_loop(1, sp_count, go, 0)
+    gate_ring.forward()
 
     own = pl.ds(pl.multiple_of(mt * tokens, tokens), tokens)
-    first, second = slots_of(routes_ref[:, own], capacity, sp_count)
     scores = scores_ref[:, own]
     most = jnp.maximum(scores[0:1, :], scores[1:2, :])
     first_exp = jnp.exp(scores[0:1, :] - most)
     second_exp = jnp.exp(scores[1:2, :] - most)
     share = group_ref[:, own] / (first_exp + second_exp)
-    slot = lax.broadcasted_iota(jnp.int32, (slots, tokens), 0)
     weights = jnp.where(slot == first, share * first_exp, 0.0)
     weights = jnp.where(slot == second, share * second_exp, weights).T
     weights_high, weights_low = halves(weights)
 
+    up_ring.forward()
+    down_a_ring.start()
     lax.fori_loop(1, sp_count, done, 0)
-    for n in range(model // piece):
-        cols = slice(n * piece, (n + 1) * piece)
-        answers = answer_ref[:, :, cols].astype(F32).reshape(slots, piece).astype(BF16)
-        mix = dot(weights_high, answers) + dot(weights_low, answers)
-        out_ref[:, cols] = (stream_ref[:, cols].astype(F32) + mix).astype(BF16)
+    gate_ring.complete()
+    up_ring.complete()
+
+    def expert(n, _):
+        rows_in = arrived_ref.reshape(slots, model)[...]
+        gated = dot(rows_in, gate_ref[n])
+        raised = dot(rows_in, up_ref[n])
+        hidden_ref[n] = (gated / (1.0 + jnp.exp(-gated)) * raised).astype(BF16)
+        return 0
+
+    lax.fori_loop(0, tp_count, expert, 0)
+
+    wide = 256
+
+    def answer(half, down_ref):
+        def some(n, _):
+            cols = pl.ds(pl.multiple_of(n * wide, wide), wide)
+            result = jnp.zeros((slots, wide), F32)
+            for quarter in range(tp_count):
+                result = result + dot(hidden_ref[quarter], down_ref[quarter, :, cols])
+            back_ref[half, :, :, cols] = result.reshape(sp_count, capacity, wide).astype(BF16)
+            return 0
+
+        lax.fori_loop(0, column_half // wide, some, 0)
+        answer_ref[half, me] = back_ref[half, me]
+
+        def go(step, _):
+            give(half, step, me).start()
+            return 0
+
+        lax.fori_loop(1, sp_count, go, 0)
+
+    def give(half, step, at):
+        peer = ring_peer(me, step, sp_count)
+        return pltpu.make_async_remote_copy(
+            src_ref=back_ref.at[half, peer],
+            dst_ref=answer_ref.at[half, peer if at is None else at],
+            send_sem=send6.at[half, peer],
+            recv_sem=recv6.at[half, peer if at is None else at],
+            device_id={"sp": peer},
+            device_id_type=MESH,
+        )
+
+    def finish(half):
+        def done(step, _):
+            give(half, step, None).wait()
+            return 0
+
+        lax.fori_loop(1, sp_count, done, 0)
+        part = answer_ref.at[half].reshape(slots, column_half)
+        for n in range(column_half // piece):
+            answers = part[:, n * piece : (n + 1) * piece]
+            mix = dot(weights_high, answers) + dot(weights_low, answers)
+            cols = slice(half * column_half + n * piece, half * column_half + (n + 1) * piece)
+            out_ref[:, cols] = (stream_ref[:, cols].astype(F32) + mix).astype(BF16)
+
+    down_a_ring.forward()
+    down_b_ring.start()
+    down_a_ring.complete()
+    answer(0, down_a_ref)
+    down_b_ring.forward()
+    down_b_ring.complete()
+    answer(1, down_b_ref)
+    finish(0)
+    finish(1)
+    for ring in (gate_ring, up_ring, down_a_ring, down_b_ring):
+        ring.sent()
 
 
 def shards(
@@ -510,43 +627,53 @@
     sp_count = lax.axis_size("sp")
     tp_count = lax.axis_size("tp")
     length, width = queries.shape
-    head_count = input_gate.shape[1]
+    head_count, head = input_gate.shape[1], head_gain.shape[1]
     tokens, model = residual.shape
     capacity = 4 * tokens // sp_count
     hidden_part = gate_weight.shape[2]
-    hidden_all = hidden_part * tp_count
-
-    gates = lax.all_gather(gate_weight[0], "tp", axis=0, tiled=False)
-    ups = lax.all_gather(up_weight[0], "tp", axis=0, tiled=False)
-    downs = lax.all_gather(down_weight[0], "tp", axis=0, tiled=True)
-
-    routes = route_experts.T
-    vmem = pl.BlockSpec(memory_space=pltpu.VMEM)
-    hbm = pl.BlockSpec(memory_space=pl.ANY)
+    planes = sp_count // PLANE
+    slots = sp_count * capacity
     dma = pltpu.SemaphoreType.DMA
-    planes = sp_count // PLANE
-    arrived, stream = pl.pallas_call(
-        functools.partial(front_kernel, sp_count, tp_count, head_count),
-        out_shape=(
-            jax.ShapeDtypeStruct((sp_count, capacity, model), BF16),
-            jax.ShapeDtypeStruct((tokens, model), BF16),
-        ),
-        in_specs=[vmem] * 7 + [hbm] + [vmem] * 3,
-        out_specs=(hbm, vmem),
+    vmem = pltpu.VMEM
+    return pl.pallas_call(
+        functools.partial(layer_kernel, sp_count, tp_count, head_count),
+        out_shape=jax.ShapeDtypeStruct((tokens, model), BF16),
+        in_specs=[pl.BlockSpec(memory_space=pl.ANY)] * 16,
+        out_specs=pl.BlockSpec(memory_space=pltpu.VMEM),
         scratch_shapes=[
-            pltpu.VMEM(output_weight.shape, BF16),
-            pltpu.VMEM((length, width), F32),
-            pltpu.VMEM((PLANE, 16, width), F32),
-            pltpu.VMEM((PLANE, 16, width), F32),
-            pltpu.VMEM((1, 16, width), F32),
-            pltpu.VMEM((planes, 16, width), F32),
-            pltpu.VMEM((PLANE, 16, width), F32),
-            pltpu.VMEM((PLANE, 16, width), F32),
-            pltpu.VMEM((tp_count, tokens, width), BF16),
-            pltpu.VMEM((tp_count, tokens, width), BF16),
-            pltpu.VMEM((sp_count, capacity, model), BF16),
-            dma,
-            dma,
+            vmem((length, width), BF16),
+            vmem((length, width), BF16),
+            vmem((length, width), BF16),
+            vmem((length, width), BF16),
+            vmem((head_count, length), F32),
+            vmem((head_count, length), F32),
+            vmem((head_count, head), F32),
+            vmem(output_weight.shape, BF16),
+            vmem((tokens, model), BF16),
+            vmem((1, model), F32),
+            vmem((2, length), jnp.int32),
+            vmem((1, length), F32),
+            vmem((2, length), F32),
+            vmem((tp_count, model, hidden_part), BF16),
+            vmem((tp_count, model, hidden_part), BF16),
+            vmem((tp_count, hidden_part, model // 2), BF16),
+            vmem((tp_count, hidden_part, model // 2), BF16),
+            vmem((length, width), F32),
+            vmem((PLANE, 16, width), F32),
+            vmem((PLANE, 16, width), F32),
+            vmem((1, 16, width), F32),
+            vmem((planes, 16, width), F32),
+            vmem((PLANE, 16, width), F32),
+            vmem((PLANE, 16, width), F32),
+            vmem((tp_count, tokens, width), BF16),
+            vmem((tp_count, tokens, width), BF16),
+            vmem((tokens, model), BF16),
+            vmem((sp_count, capacity, model), BF16),
+            vmem((sp_count, capacity, model), BF16),
+            vmem((tp_count, slots, hidden_part), BF16),
+            vmem((2, sp_count, capacity, model // 2), BF16),
+            vmem((2, sp_count, capacity, model // 2), BF16),
+            dma((17,)),
             dma((PLANE,)),
             dma((PLANE,)),
             dma((planes,)),
@@ -557,12 +684,13 @@
             dma((tp_count,)),
             dma((sp_count,)),
             dma((sp_count,)),
+            dma((2, sp_count)),
+            dma((2, sp_count)),
+            dma((4, 4)),
+            dma((4, 4)),
         ],
         compiler_params=pltpu.CompilerParams(
-            collective_id=0, has_side_effects=True, vmem_limit_bytes=40 * 2**20
-        ),
-        cost_estimate=pl.CostEstimate(
-            flops=60_000_000_000, bytes_accessed=10_000_000, transcendentals=0
+            collective_id=0, has_side_effects=True, vmem_limit_bytes=66_000_000
         ),
     )(
         queries,
@@ -571,50 +699,17 @@
         output_gate,
         input_gate.T,
         forget_gate.T,
-        head_gain.reshape(1, width),
+        head_gain,
         output_weight,
         residual,
         norm_gain.reshape(1, model),
-        routes,
+        route_experts.T,
+        group_weight.reshape(1, length),
+        expert_scores.T,
+        gate_weight,
+        up_weight,
+        down_weight,
     )
-
-    slots = sp_count * capacity
-    hidden = pl.pallas_call(
-        hidden_kernel,
-        grid=(tp_count,),
-        out_shape=jax.ShapeDtypeStruct((slots, hidden_all), BF16),
-        in_specs=[
-            pl.BlockSpec((slots, model), lambda n: (0, 0)),
-            pl.BlockSpec((1, model, hidden_part), lambda n: (n, 0, 0)),
-            pl.BlockSpec((1, model, hidden_part), lambda n: (n, 0, 0)),
-        ],
-        out_specs=pl.BlockSpec((slots, hidden_part), lambda n: (0, n)),
-        compiler_params=pltpu.CompilerParams(vmem_limit_bytes=40 * 2**20),
-        cost_estimate=pl.CostEstimate(
-            flops=4 * slots * model * hidden_all,
-            bytes_accessed=4 * model * hidden_all,
-            transcendentals=slots * hidden_all,
-        ),
-    )(arrived.reshape(slots, model), gates, ups)
-
-    return pl.pallas_call(
-        functools.partial(back_kernel, sp_count, tp_count),
-        out_shape=jax.ShapeDtypeStruct((tokens, model), BF16),
-        in_specs=[vmem] * 6,
-        out_specs=vmem,
-        scratch_shapes=[
-            pltpu.VMEM((sp_count, capacity, model), BF16),
-            pltpu.VMEM((sp_count, capacity, model), BF16),
-            dma((sp_count,)),
-            dma((sp_count,)),
-        ],
-        compiler_params=pltpu.CompilerParams(
-            collective_id=1, has_side_effects=True, vmem_limit_bytes=40 * 2**20
-        ),
-        cost_estimate=pl.CostEstimate(
-            flops=60_000_000_000, bytes_accessed=10_000_000, transcendentals=0
-        ),
-    )(hidden, downs, stream, routes, group_weight.reshape(1, length), expert_scores.T)
 
 
 def solution(mesh):

time: 241 us -> 159 us (0.66)
  waiting for transfers between devices: 57.9 us -> 0 us
  local copies, waits for them, and re-layouts: 19.8 us -> 1.88 us
  between operations: 13.2 us -> 0.01 us
  Pallas kernels: 150 us -> 157 us
    all_gather x3 -> x0, waiting for transfers between devices: 55.8 us -> none  [the longest x1 43.3 us: shards(): downs = lax.all_gather(down_weight[0], 'tp', axis=0, tiled=True)]
    unnamed x37 -> x1, local copies, waits for them, and re-layouts: 19 us -> 1.88 us
    pallas_call x3 -> x1, Pallas kernels: 150 us -> 157 us  [shards(): pl.pallas_call(functools.partial(layer_kernel, sp_count, tp_count, head_c...]
  transfers between devices with their start and end apart: 3 -> 0, of which waited for: 2 -> 0; matrix products, arithmetic and copies ran while one was open for 0% -> 0% of each run, Pallas kernels for 38% -> 0%
where the time goes in v2:
time: 159 us
  Pallas kernels  157 us (99%)
  local copies, waits for them, and re-layouts  1.88 us (1%)
    pallas_call x1, Pallas kernels, shards(): pl.pallas_call(functools.partial(layer_kernel, sp_count, tp_count, head_c...  157 us

profile of v2, /device:TPU:1, one launch (start us, length us, event | category | flops | bytes accessed | tf_op | source)
XLA Modules:
  0.0 158.8 jit_solution(1826308012145743027)
XLA Ops:
  0.0 156.9 %shard_map.154 = bf16[128,2048]{1,0:T(8,128)(2,1)} custom-call(bf16[512,256]{1,0:T(8,128)(2,1)} %refs_0_.1, bf16[512,256]{1,0:T(8,128)(2,1)} %refs_1_.1, bf16[512,256]{1,0:T(8,128)(2,1)} %refs_2_.1, bf16[512,256]{1,0:T(8,128)(2,1)} %refs_3_.1, f32[4,512]{1,0:T(4,128)} %bitcast.6, f32[4,512]{1,0:T(4,128)} %bitcast.7, f32[4,64]{1,0:T(4,128)} %refs_6_.1, ...), custom_call_target="tpu_custom_call" | custom-call | tf_op jit(solution)/shard_map/pallas_call | solution.py:638
  156.9 1.9 %copy.18 = bf16[128,2048]{1,0:T(8,128)(2,1)} copy(bf16[128,2048]{1,0:T(8,128)(2,1)} %shard_map.154) | data formatting | bytes 1048576

commit v3 on v2

--- a/solution.py
+++ b/solution.py
@@ -11,6 +11,7 @@
 VERY_NEGATIVE = -1e30
 MESH = pl.DeviceIdType.MESH
 PLANE = 8
+WIDTHS = (256, 256, 512, 512, 512)
 F32 = jnp.float32
 BF16 = jnp.bfloat16
 
@@ -71,6 +72,12 @@
     away = (step + 1) // 2
     sign = 2 * lax.rem(step, 2) - 1
     return lax.rem(me + sign * away + count, count)
+
+
+def ring_source(me, step, count):
+    away = (step + 1) // 2
+    sign = 2 * lax.rem(step, 2) - 1
+    return lax.rem(me - sign * away + count, count)
 
 
 def slots_of(routes, capacity, experts):
@@ -158,6 +165,12 @@
 
 
 def layer_kernel(sp_count, tp_count, head_count, *refs):
+    chunks = len(WIDTHS)
+    starts = [sum(WIDTHS[:n]) for n in range(chunks)]
+    listed = refs[len(refs) - 3 * chunks :]
+    refs = refs[: len(refs) - 3 * chunks]
+    back_refs, answer_refs = listed[:chunks], listed[chunks : 2 * chunks]
+    down_refs = listed[2 * chunks :]
     (
         q_hbm,
         k_hbm,
@@ -191,9 +204,8 @@
         scores_ref,
         gate_ref,
         up_ref,
-        down_a_ref,
-        down_b_ref,
         intra_ref,
+        peak_ref,
         s1_ref,
         r1_ref,
         s2_ref,
@@ -206,8 +218,6 @@
         send_ref,
         arrived_ref,
         hidden_ref,
-        back_ref,
-        answer_ref,
         load_sem,
         send1,
         recv1,
@@ -235,7 +245,8 @@
     capacity = send_ref.shape[1]
     model = send_ref.shape[2]
     slots = sp_count * capacity
-    column_half = model // 2
+
+    barrier = pltpu.get_barrier_semaphore()
 
     loads = [
         (fg_hbm, fg_ref),
@@ -253,39 +264,31 @@
         (res_hbm, res_ref),
         (up_hbm.at[0], up_ref.at[mt]),
         (wo_hbm, wo_ref),
-        (down_hbm.at[0, :, pl.ds(0, column_half)], down_a_ref.at[mt]),
-        (down_hbm.at[0, :, pl.ds(column_half, column_half)], down_b_ref.at[mt]),
     ]
+    for start, size, ref in zip(starts, WIDTHS, down_refs):
+        loads.append((down_hbm.at[0, :, pl.ds(start, size)], ref.at[mt]))
     loads = [
         pltpu.make_async_copy(source, target, load_sem.at[n])
         for n, (source, target) in enumerate(loads)
     ]
-    for load in loads:
+    for load in loads[:6]:
         load.start()
 
-    barrier = pltpu.get_barrier_semaphore()
-
-    def greet(step, _):
-        pl.semaphore_signal(
-            barrier, inc=1, device_id={"sp": ring_peer(me, step, sp_count)}, device_id_type=MESH
-        )
-        return 0
-
-    lax.fori_loop(1, sp_count, greet, 0)
-
-    def greet_tp(step, _):
-        pl.semaphore_signal(
-            barrier, inc=1, device_id={"tp": lax.rem(mt + step, tp_count)}, device_id_type=MESH
-        )
-        return 0
-
-    lax.fori_loop(1, tp_count, greet_tp, 0)
-
-    gate_ring, up_ring, down_a_ring, down_b_ring = [
+    for step in range(1, PLANE):
+        peer = zed * PLANE + lax.rem(place + step, PLANE)
+        pl.semaphore_signal(barrier, inc=1, device_id={"sp": peer}, device_id_type=MESH)
+    for step in range(1, planes):
+        peer = lax.rem(zed + step, planes) * PLANE + place
+        pl.semaphore_signal(barrier, inc=1, device_id={"sp": peer}, device_id_type=MESH)
+    for step in range(1, tp_count):
+        peer = lax.rem(mt + step, tp_count)
+        pl.semaphore_signal(barrier, inc=1, device_id={"tp": peer}, device_id_type=MESH)
+
+    gate_ring, up_ring, *down_rings = [
         Ring(ref, item, mt, tp_count, ring_send, ring_recv)
-        for item, ref in enumerate((gate_ref, up_ref, down_a_ref, down_b_ref))
+        for item, ref in enumerate((gate_ref, up_ref, *down_refs))
     ]
-    for load in loads[:6]:
+    for load in loads[:5]:
         load.wait()
 
     small = jnp.exp(-fg_ref[...])
@@ -325,60 +328,65 @@
         put(s1_ref, n, (total_row, level_row, memory[n * rows : (n + 1) * rows, :]))
     put(r1_ref, place, unpacked(s1_ref, place))
 
-    pl.semaphore_wait(barrier, sp_count - 1 + tp_count - 1)
+    pl.semaphore_wait(barrier, PLANE + planes + tp_count - 3)
+    loads[5].wait()
+
+    def whole(source, landed, send_sem, recv_sem):
+        return pltpu.make_async_remote_copy(
+            src_ref=source,
+            dst_ref=landed,
+            send_sem=send_sem,
+            recv_sem=recv_sem,
+            device_id={"tp": lax.rem(mt + 1, tp_count)},
+            device_id_type=MESH,
+        )
 
     def exchange1(step):
         peer = lax.rem(place + step, PLANE)
         return pltpu.make_async_remote_copy(
             src_ref=s1_ref.at[peer],
             dst_ref=r1_ref.at[place],
-            send_sem=send1.at[peer],
-            recv_sem=recv1.at[place],
+            send_sem=send1,
+            recv_sem=recv1,
             device_id={"sp": zed * PLANE + peer},
             device_id_type=MESH,
         )
 
-    def arrival1(step):
+    def exchange2(step):
+        peer = lax.rem(zed + step, planes)
+        return pltpu.make_async_remote_copy(
+            src_ref=s2_ref.at[0],
+            dst_ref=r2_ref.at[zed],
+            send_sem=send2,
+            recv_sem=recv2,
+            device_id={"sp": peer * PLANE + place},
+            device_id_type=MESH,
+        )
+
+    def exchange3(step):
         peer = lax.rem(place + step, PLANE)
         return pltpu.make_async_remote_copy(
-            src_ref=s1_ref.at[peer],
-            dst_ref=r1_ref.at[peer],
-            send_sem=send1.at[peer],
-            recv_sem=recv1.at[peer],
+            src_ref=s3_ref.at[peer],
+            dst_ref=r3_ref.at[place],
+            send_sem=send3,
+            recv_sem=recv3,
             device_id={"sp": zed * PLANE + peer},
             device_id_type=MESH,
         )
 
-    def exchange2(step, at):
-        peer = lax.rem(zed + step, planes)
-        return pltpu.make_async_remote_copy(
-            src_ref=s2_ref.at[0],
-            dst_ref=r2_ref.at[peer if at is None else at],
-            send_sem=send2.at[peer],
-            recv_sem=recv2.at[peer if at is None else at],
-            device_id={"sp": peer * PLANE + place},
-            device_id_type=MESH,
-        )
-
-    def exchange3(step, at):
-        peer = lax.rem(place + step, PLANE)
-        return pltpu.make_async_remote_copy(
-            src_ref=s3_ref.at[peer],
-            dst_ref=r3_ref.at[peer if at is None else at],
-            send_sem=send3.at[peer],
-            recv_sem=recv3.at[peer if at is None else at],
-            device_id={"sp": zed * PLANE + peer},
-            device_id_type=MESH,
-        )
-
+    rest = pl.ds(0, PLANE - 1)
+    rest_planes = pl.ds(0, planes - 1)
     for step in range(1, PLANE):
         exchange1(step).start()
     gate_ring.start()
+    for load in loads[6:]:
+        load.start()
 
     peak_cols = jnp.concatenate([peak, jnp.zeros((8 - head_count, length), F32)], axis=0).T
     peak_wide = jnp.zeros((length, width), F32)
     for h in range(head_count):
         peak_wide = jnp.where(masks[h], peak_cols[:, h : h + 1], peak_wide)
+    peak_ref[...] = peak_wide
     scale = head**-0.5
     block = 128
 
@@ -403,8 +411,7 @@
     inner(0)
     inner(1)
 
-    for step in range(1, PLANE):
-        arrival1(step).wait()
+    whole(s1_ref.at[rest], r1_ref.at[rest], send1, recv1).wait()
     identity = (
         jnp.zeros((1, width), F32),
         jnp.full((1, width), VERY_NEGATIVE, F32),
@@ -416,12 +423,11 @@
     put(s2_ref, 0, prior[-1])
     put(r2_ref, zed, prior[-1])
     for step in range(1, planes):
-        exchange2(step, zed).start()
+        exchange2(step).start()
 
     inner(2)
 
-    for step in range(1, planes):
-        exchange2(step, None).wait()
+    whole(r2_ref.at[rest_planes], r2_ref.at[rest_planes], send2, recv2).wait()
     entering = identity
     for n in range(planes):
         later = join(entering, unpacked(r2_ref, n))
@@ -430,12 +436,11 @@
         put(s3_ref, n, join(entering, prior[n]))
     put(r3_ref, place, unpacked(s3_ref, place))
     for step in range(1, PLANE):
-        exchange3(step, place).start()
+        exchange3(step).start()
 
     inner(3)
 
-    for step in range(1, PLANE):
-        exchange3(step, None).wait()
+    whole(s3_ref.at[rest], r3_ref.at[rest], send3, recv3).wait()
     prior_total = r3_ref[0, 8:9, :]
     prior_level = r3_ref[0, 9:10, :]
     start_level = jnp.maximum(prior_level, prior_total)
@@ -443,46 +448,51 @@
     began = jnp.concatenate([r3_ref[n, 0:8, :] for n in range(PLANE)], axis=0) * opening
     blocks = jnp.concatenate([jnp.where(masks[h], began, 0.0) for h in range(head_count)], axis=0)
     block_high, block_low = halves(blocks)
-    queries = (q_ref[...].astype(F32) * scale).astype(BF16)
-    carried = dot(queries, block_high) + dot(queries, block_low)
-    level = jnp.maximum(peak_wide, start_level)
-    cell = jnp.exp(peak_wide - level) * intra_ref[...] + jnp.exp(start_level - level) * carried
     row_head = lax.broadcasted_iota(jnp.int32, (width, width), 0) // head
     column_head = lax.broadcasted_iota(jnp.int32, (width, width), 1) // head
     averaging = jnp.where(row_head == column_head, 1.0 / head, 0.0).astype(BF16)
-    square_high, square_low = halves(cell * cell)
-    mean = dot(square_high, averaging) + dot(square_low, averaging)
     for load in loads[6:]:
         load.wait()
     gain = jnp.concatenate([hgain_ref[h : h + 1, :] for h in range(head_count)], axis=1)
-    gate = 1.0 / (1.0 + jnp.exp(-og_ref[...].astype(F32)))
-    mixed = (gate * (cell * lax.rsqrt(mean + EPSILON) * gain)).astype(BF16)
-    for n in range(tp_count):
-        mix_ref[n] = mixed[n * tokens : (n + 1) * tokens, :]
-
-    def exchange4(step, at):
+
+    def exchange4(step):
         peer = lax.rem(mt + step, tp_count)
         return pltpu.make_async_remote_copy(
             src_ref=mix_ref.at[peer],
-            dst_ref=mrecv_ref.at[peer if at is None else at],
-            send_sem=send4.at[peer],
-            recv_sem=recv4.at[peer if at is None else at],
+            dst_ref=mrecv_ref.at[mt],
+            send_sem=send4,
+            recv_sem=recv4,
             device_id={"tp": peer},
             device_id_type=MESH,
         )
 
-    for step in range(1, tp_count):
-        exchange4(step, mt).start()
+    for step in (2, 1, 3, 0):
+        peer = lax.rem(mt + step, tp_count)
+        rows_t = pl.ds(pl.multiple_of(peer * tokens, tokens), tokens)
+        queries = (q_ref[rows_t, :].astype(F32) * scale).astype(BF16)
+        carried = dot(queries, block_high) + dot(queries, block_low)
+        peak_wide = peak_ref[rows_t, :]
+        level = jnp.maximum(peak_wide, start_level)
+        cell = jnp.exp(peak_wide - level) * intra_ref[rows_t, :]
+        cell = cell + jnp.exp(start_level - level) * carried
+        square_high, square_low = halves(cell * cell)
+        mean = dot(square_high, averaging) + dot(square_low, averaging)
+        gate = 1.0 / (1.0 + jnp.exp(-og_ref[rows_t, :].astype(F32)))
+        mixed = (gate * (cell * lax.rsqrt(mean + EPSILON) * gain)).astype(BF16)
+        if step:
+            mix_ref[peer] = mixed
+            exchange4(step).start()
+        else:
+            mrecv_ref[mt] = mixed
     up_ring.start()
-    mrecv_ref[mt] = mix_ref[mt]
 
     routes = routes_ref[:, pl.ds(pl.multiple_of(mt * tokens, tokens), tokens)]
     first, second = slots_of(routes, capacity, sp_count)
     slot = lax.broadcasted_iota(jnp.int32, (slots, tokens), 0)
     select = jnp.where((slot == first) | (slot == second), 1.0, 0.0).astype(BF16)
 
-    for step in range(1, tp_count):
-        exchange4(step, None).wait()
+    others = pl.ds(0, tp_count - 1)
+    whole(mix_ref.at[others], mrecv_ref.at[others], send4, recv4).wait()
     gathered = jnp.concatenate([mrecv_ref[n] for n in range(tp_count)], axis=1)
     piece = 512
     squares = jnp.zeros((tokens, 1), F32)
@@ -500,25 +510,23 @@
         chosen = dot(select, normed).reshape(sp_count, capacity, piece)
         send_ref[:, :, cols] = chosen.astype(BF16)
 
-    arrived_ref[me] = send_ref[me]
-
-    def dispatch(step, at):
+    arrived_ref[0] = send_ref[me]
+    row_parts = 2
+    group = sp_count // row_parts
+
+    def dispatch(step):
         peer = ring_peer(me, step, sp_count)
         return pltpu.make_async_remote_copy(
             src_ref=send_ref.at[peer],
-            dst_ref=arrived_ref.at[peer if at is None else at],
-            send_sem=send5.at[peer],
-            recv_sem=recv5.at[peer if at is None else at],
+            dst_ref=arrived_ref.at[step],
+            send_sem=send5,
+            recv_sem=recv5.at[step // group],
             device_id={"sp": peer},
             device_id_type=MESH,
         )
 
     def go(step, _):
-        dispatch(step, me).start()
-        return 0
-
-    def done(step, _):
-        dispatch(step, None).wait()
+        dispatch(step).start()
         return 0
 
     lax.fori_loop(1, sp_count, go, 0)
@@ -535,74 +543,81 @@
     weights_high, weights_low = halves(weights)
 
     up_ring.forward()
-    down_a_ring.start()
-    lax.fori_loop(1, sp_count, done, 0)
+    down_rings[0].start()
+    down_rings[1].start()
+
+    many = slots // row_parts
+    rows_in = arrived_ref.reshape(slots, model)
+
+    def expert(part, quarter):
+        rows_t = slice(part * many, (part + 1) * many)
+        gated = dot(rows_in[rows_t, :], gate_ref[quarter])
+        raised = dot(rows_in[rows_t, :], up_ref[quarter])
+        hidden_ref[quarter, rows_t, :] = (gated / (1.0 + jnp.exp(-gated)) * raised).astype(BF16)
+
+    for part in range(row_parts):
+        landed = arrived_ref.at[pl.ds(part * group, group - (part == 0))]
+        whole(landed, landed, send5, recv5.at[part]).wait_recv()
+
+        def near(n, _):
+            expert(part, lax.rem(mt + n + tp_count - 1, tp_count))
+            return 0
+
+        lax.fori_loop(0, 3, near, 0)
     gate_ring.complete()
     up_ring.complete()
-
-    def expert(n, _):
-        rows_in = arrived_ref.reshape(slots, model)[...]
-        gated = dot(rows_in, gate_ref[n])
-        raised = dot(rows_in, up_ref[n])
-        hidden_ref[n] = (gated / (1.0 + jnp.exp(-gated)) * raised).astype(BF16)
-        return 0
-
-    lax.fori_loop(0, tp_count, expert, 0)
+    for part in range(row_parts):
+        expert(part, lax.rem(mt + 2, tp_count))
 
     wide = 256
 
-    def answer(half, down_ref):
-        def some(n, _):
-            cols = pl.ds(pl.multiple_of(n * wide, wide), wide)
+    def give(chunk, step):
+        peer = ring_source(me, step, sp_count)
+        return pltpu.make_async_remote_copy(
+            src_ref=back_refs[chunk].at[step],
+            dst_ref=answer_refs[chunk].at[me],
+            send_sem=send6.at[chunk],
+            recv_sem=recv6.at[chunk],
+            device_id={"sp": peer},
+            device_id_type=MESH,
+        )
+
+    def answer(chunk):
+        down_ref, back_ref = down_refs[chunk], back_refs[chunk]
+        for n in range(WIDTHS[chunk] // wide):
+            cols = slice(n * wide, (n + 1) * wide)
             result = jnp.zeros((slots, wide), F32)
             for quarter in range(tp_count):
                 result = result + dot(hidden_ref[quarter], down_ref[quarter, :, cols])
-            back_ref[half, :, :, cols] = result.reshape(sp_count, capacity, wide).astype(BF16)
+            back_ref[:, :, cols] = result.reshape(sp_count, capacity, wide).astype(BF16)
+        answer_refs[chunk][me] = back_ref[0]
+
+        def go(step, _):
+            give(chunk, step).start()
             return 0
 
-        lax.fori_loop(0, column_half // wide, some, 0)
-        answer_ref[half, me] = back_ref[half, me]
-
-        def go(step, _):
-            give(half, step, me).start()
-            return 0
-
         lax.fori_loop(1, sp_count, go, 0)
 
-    def give(half, step, at):
-        peer = ring_peer(me, step, sp_count)
-        return pltpu.make_async_remote_copy(
-            src_ref=back_ref.at[half, peer],
-            dst_ref=answer_ref.at[half, peer if at is None else at],
-            send_sem=send6.at[half, peer],
-            recv_sem=recv6.at[half, peer if at is None else at],
-            device_id={"sp": peer},
-            device_id_type=MESH,
-        )
-
-    def finish(half):
-        def done(step, _):
-            give(half, step, None).wait()
-            return 0
-
-        lax.fori_loop(1, sp_count, done, 0)
-        part = answer_ref.at[half].reshape(slots, column_half)
-        for n in range(column_half // piece):
-            answers = part[:, n * piece : (n + 1) * piece]
-            mix = dot(weights_high, answers) + dot(weights_low, answers)
-            cols = slice(half * column_half + n * piece, half * column_half + (n + 1) * piece)
-            out_ref[:, cols] = (stream_ref[:, cols].astype(F32) + mix).astype(BF16)
-
-    down_a_ring.forward()
-    down_b_ring.start()
-    down_a_ring.complete()
-    answer(0, down_a_ref)
-    down_b_ring.forward()
-    down_b_ring.complete()
-    answer(1, down_b_ref)
-    finish(0)
-    finish(1)
-    for ring in (gate_ring, up_ring, down_a_ring, down_b_ring):
+    def finish(chunk):
+        back, landed = back_refs[chunk], answer_refs[chunk]
+        most_of = pl.ds(0, sp_count - 1)
+        whole(back.at[most_of], landed.at[most_of], send6.at[chunk], recv6.at[chunk]).wait()
+        answers = answer_refs[chunk].reshape(slots, WIDTHS[chunk])[...]
+        mix = dot(weights_high, answers) + dot(weights_low, answers)
+        cols = slice(starts[chunk], starts[chunk] + WIDTHS[chunk])
+        out_ref[:, cols] = (stream_ref[:, cols].astype(F32) + mix).astype(BF16)
+
+    for chunk in range(chunks):
+        down_rings[chunk].forward()
+        if chunk + 2 < chunks:
+            down_rings[chunk + 2].start()
+        down_rings[chunk].complete()
+        answer(chunk)
+    for chunk in range(chunks):
+        finish(chunk)
+    left = send_ref.at[pl.ds(0, sp_count - 1)]
+    whole(left, left, send5, recv5.at[0]).wait_send()
+    for ring in (gate_ring, up_ring, *down_rings):
         ring.sent()
 
 
@@ -656,8 +671,7 @@
             vmem((2, length), F32),
             vmem((tp_count, model, hidden_part), BF16),
             vmem((tp_count, model, hidden_part), BF16),
-            vmem((tp_count, hidden_part, model // 2), BF16),
-            vmem((tp_count, hidden_part, model // 2), BF16),
+            vmem((length, width), F32),
             vmem((length, width), F32),
             vmem((PLANE, 16, width), F32),
             vmem((PLANE, 16, width), F32),
@@ -671,23 +685,24 @@
             vmem((sp_count, capacity, model), BF16),
             vmem((sp_count, capacity, model), BF16),
             vmem((tp_count, slots, hidden_part), BF16),
-            vmem((2, sp_count, capacity, model // 2), BF16),
-            vmem((2, sp_count, capacity, model // 2), BF16),
-            dma((17,)),
-            dma((PLANE,)),
-            dma((PLANE,)),
-            dma((planes,)),
-            dma((planes,)),
-            dma((PLANE,)),
-            dma((PLANE,)),
-            dma((tp_count,)),
-            dma((tp_count,)),
-            dma((sp_count,)),
-            dma((sp_count,)),
-            dma((2, sp_count)),
-            dma((2, sp_count)),
-            dma((4, 4)),
-            dma((4, 4)),
+            dma((15 + len(WIDTHS),)),
+            dma,
+            dma,
+            dma,
+            dma,
+            dma,
+            dma,
+            dma,
+            dma,
+            dma,
+            dma((2,)),
+            dma((len(WIDTHS),)),
+            dma((len(WIDTHS),)),
+            dma((2 + len(WIDTHS), 4)),
+            dma((2 + len(WIDTHS), 4)),
+            *[vmem((sp_count, capacity, n), BF16) for n in WIDTHS],
+            *[vmem((sp_count, capacity, n), BF16) for n in WIDTHS],
+            *[vmem((tp_count, hidden_part, n), BF16) for n in WIDTHS],
         ],
         compiler_params=pltpu.CompilerParams(
             collective_id=0, has_side_effects=True, vmem_limit_bytes=66_000_000

time: 159 us -> 150 us (0.943)
  Pallas kernels: 157 us -> 148 us
    pallas_call x1, Pallas kernels: 157 us -> 148 us  [shards(): pl.pallas_call(functools.partial(layer_kernel, sp_count, tp_count, head_c...]
where the time goes in v3:
time: 150 us
  Pallas kernels  148 us (99%)
  local copies, waits for them, and re-layouts  1.88 us (1%)
    pallas_call x1, Pallas kernels, shards(): pl.pallas_call(functools.partial(layer_kernel, sp_count, tp_count, head_c...  148 us

profile of v3, /device:TPU:1, one launch (start us, length us, event | category | flops | bytes accessed | tf_op | source)
XLA Modules:
  0.0 150.1 jit_solution(13048917542996415843)
XLA Ops:
  0.0 148.2 %shard_map.154 = bf16[128,2048]{1,0:T(8,128)(2,1)} custom-call(bf16[512,256]{1,0:T(8,128)(2,1)} %refs_0_.1, bf16[512,256]{1,0:T(8,128)(2,1)} %refs_1_.1, bf16[512,256]{1,0:T(8,128)(2,1)} %refs_2_.1, bf16[512,256]{1,0:T(8,128)(2,1)} %refs_3_.1, f32[4,512]{1,0:T(4,128)} %bitcast.6, f32[4,512]{1,0:T(4,128)} %bitcast.7, f32[4,64]{1,0:T(4,128)} %refs_6_.1, ...), custom_call_target="tpu_custom_call" | custom-call | tf_op jit(solution)/shard_map/pallas_call | solution.py:653
  148.2 1.9 %copy.18 = bf16[128,2048]{1,0:T(8,128)(2,1)} copy(bf16[128,2048]{1,0:T(8,128)(2,1)} %shard_map.154) | data formatting | bytes 1048576

commit v4 on v3

--- a/solution.py
+++ b/solution.py
@@ -11,7 +11,7 @@
 VERY_NEGATIVE = -1e30
 MESH = pl.DeviceIdType.MESH
 PLANE = 8
-WIDTHS = (256, 256, 512, 512, 512)
+WIDTHS = (256, 256, 256, 256, 512, 512)
 F32 = jnp.float32
 BF16 = jnp.bfloat16
 
@@ -53,19 +53,16 @@
     return early_total + late_total, level, memory
 
 
-def packed(total, level, memory):
-    row = lax.broadcasted_iota(jnp.int32, memory.shape, 0)
-    return memory, jnp.where(row == 0, total, jnp.where(row == 1, level, 0.0))
-
-
-def unpacked(ref, index):
-    return ref[index, 8:9, :], ref[index, 9:10, :], ref[index, 0:8, :]
-
-
-def put(ref, index, state):
-    memory, scalars = packed(*state)
-    ref[index, 0:8, :] = memory
-    ref[index, 8:16, :] = scalars
+def unpacked(memory_ref, scalars_ref, index):
+    scalars = scalars_ref[index]
+    return scalars[0:1, :], scalars[1:2, :], memory_ref[index]
+
+
+def put(memory_ref, scalars_ref, index, state):
+    total, level, memory = state
+    memory_ref[index] = memory
+    scalars_ref[index, 0:1, :] = total
+    scalars_ref[index, 1:2, :] = level
 
 
 def ring_peer(me, step, count):
@@ -207,9 +204,13 @@
         intra_ref,
         peak_ref,
         s1_ref,
+        s1s_ref,
         r1_ref,
+        r1s_ref,
         s2_ref,
+        s2s_ref,
         r2_ref,
+        r2s_ref,
         s3_ref,
         r3_ref,
         mix_ref,
@@ -221,8 +222,12 @@
         load_sem,
         send1,
         recv1,
+        send1s,
+        recv1s,
         send2,
         recv2,
+        send2s,
+        recv2s,
         send3,
         recv3,
         send4,
@@ -284,9 +289,12 @@
         peer = lax.rem(mt + step, tp_count)
         pl.semaphore_signal(barrier, inc=1, device_id={"tp": peer}, device_id_type=MESH)
 
-    gate_ring, up_ring, *down_rings = [
+    early = 3 * model // 4
+    gate_first = gate_ref.at[:, pl.ds(0, early), :]
+    gate_last = gate_ref.at[:, pl.ds(early, model - early), :]
+    gate_ring, gate_rest, up_ring, *down_rings = [
         Ring(ref, item, mt, tp_count, ring_send, ring_recv)
-        for item, ref in enumerate((gate_ref, up_ref, *down_refs))
+        for item, ref in enumerate((gate_first, gate_last, up_ref, *down_refs))
     ]
     for load in loads[:5]:
         load.wait()
@@ -325,8 +333,11 @@
         memory = jnp.where(masks[h], whole[h * head : (h + 1) * head, :], memory)
     rows = head // PLANE
     for n in range(PLANE):
-        put(s1_ref, n, (total_row, level_row, memory[n * rows : (n + 1) * rows, :]))
-    put(r1_ref, place, unpacked(s1_ref, place))
+        s1_ref[n] = memory[n * rows : (n + 1) * rows, :]
+    s1s_ref[0, 0:1, :] = total_row
+    s1s_ref[0, 1:2, :] = level_row
+    r1_ref[place] = s1_ref[place]
+    r1s_ref[place] = s1s_ref[0]
 
     pl.semaphore_wait(barrier, PLANE + planes + tp_count - 3)
     loads[5].wait()
@@ -352,6 +363,28 @@
             device_id_type=MESH,
         )
 
+    def exchange1s(step):
+        peer = lax.rem(place + step, PLANE)
+        return pltpu.make_async_remote_copy(
+            src_ref=s1s_ref.at[0],
+            dst_ref=r1s_ref.at[place],
+            send_sem=send1s,
+            recv_sem=recv1s,
+            device_id={"sp": zed * PLANE + peer},
+            device_id_type=MESH,
+        )
+
+    def exchange2s(step):
+        peer = lax.rem(zed + step, planes)
+        return pltpu.make_async_remote_copy(
+            src_ref=s2s_ref.at[0],
+            dst_ref=r2s_ref.at[zed],
+            send_sem=send2s,
+            recv_sem=recv2s,
+            device_id={"sp": peer * PLANE + place},
+            device_id_type=MESH,
+        )
+
     def exchange2(step):
         peer = lax.rem(zed + step, planes)
         return pltpu.make_async_remote_copy(
@@ -377,6 +410,7 @@
     rest = pl.ds(0, PLANE - 1)
     rest_planes = pl.ds(0, planes - 1)
     for step in range(1, PLANE):
+        exchange1s(step).start()
         exchange1(step).start()
     gate_ring.start()
     for load in loads[6:]:
@@ -411,7 +445,8 @@
     inner(0)
     inner(1)
 
-    whole(s1_ref.at[rest], r1_ref.at[rest], send1, recv1).wait()
+    whole(r1s_ref.at[rest], r1s_ref.at[rest], send1s, recv1s).wait()
+    whole(r1_ref.at[rest], r1_ref.at[rest], send1, recv1).wait()
     identity = (
         jnp.zeros((1, width), F32),
         jnp.full((1, width), VERY_NEGATIVE, F32),
@@ -419,33 +454,37 @@
     )
     prior = [identity]
     for n in range(PLANE):
-        prior.append(join(prior[-1], unpacked(r1_ref, n)))
-    put(s2_ref, 0, prior[-1])
-    put(r2_ref, zed, prior[-1])
+        prior.append(join(prior[-1], unpacked(r1_ref, r1s_ref, n)))
+    put(s2_ref, s2s_ref, 0, prior[-1])
+    put(r2_ref, r2s_ref, zed, prior[-1])
     for step in range(1, planes):
+        exchange2s(step).start()
         exchange2(step).start()
 
     inner(2)
 
+    whole(r2s_ref.at[rest_planes], r2s_ref.at[rest_planes], send2s, recv2s).wait()
     whole(r2_ref.at[rest_planes], r2_ref.at[rest_planes], send2, recv2).wait()
     entering = identity
     for n in range(planes):
-        later = join(entering, unpacked(r2_ref, n))
+        later = join(entering, unpacked(r2_ref, r2s_ref, n))
         entering = tuple(jnp.where(n < zed, new, old) for new, old in zip(later, entering))
+    prior_total, prior_level, _ = identity
     for n in range(PLANE):
-        put(s3_ref, n, join(entering, prior[n]))
-    put(r3_ref, place, unpacked(s3_ref, place))
+        total, level, part = join(entering, prior[n])
+        s3_ref[n] = part
+        prior_total = jnp.where(place == n, total, prior_total)
+        prior_level = jnp.where(place == n, level, prior_level)
+    r3_ref[place] = s3_ref[place]
     for step in range(1, PLANE):
         exchange3(step).start()
 
     inner(3)
 
     whole(s3_ref.at[rest], r3_ref.at[rest], send3, recv3).wait()
-    prior_total = r3_ref[0, 8:9, :]
-    prior_level = r3_ref[0, 9:10, :]
     start_level = jnp.maximum(prior_level, prior_total)
     opening = jnp.exp(prior_level - start_level)
-    began = jnp.concatenate([r3_ref[n, 0:8, :] for n in range(PLANE)], axis=0) * opening
+    began = jnp.concatenate([r3_ref[n] for n in range(PLANE)], axis=0) * opening
     blocks = jnp.concatenate([jnp.where(masks[h], began, 0.0) for h in range(head_count)], axis=0)
     block_high, block_low = halves(blocks)
     row_head = lax.broadcasted_iota(jnp.int32, (width, width), 0) // head
@@ -484,6 +523,7 @@
             exchange4(step).start()
         else:
             mrecv_ref[mt] = mixed
+    gate_rest.start()
     up_ring.start()
 
     routes = routes_ref[:, pl.ds(pl.multiple_of(mt * tokens, tokens), tokens)]
@@ -531,6 +571,8 @@
 
     lax.fori_loop(1, sp_count, go, 0)
     gate_ring.forward()
+    gate_rest.forward()
+    down_rings[0].start()
 
     own = pl.ds(pl.multiple_of(mt * tokens, tokens), tokens)
     scores = scores_ref[:, own]
@@ -543,8 +585,6 @@
     weights_high, weights_low = halves(weights)
 
     up_ring.forward()
-    down_rings[0].start()
-    down_rings[1].start()
 
     many = slots // row_parts
     rows_in = arrived_ref.reshape(slots, model)
@@ -564,7 +604,12 @@
             return 0
 
         lax.fori_loop(0, 3, near, 0)
+        if part == 0:
+            down_rings[0].forward()
+            down_rings[1].start()
+            down_rings[2].start()
     gate_ring.complete()
+    gate_rest.complete()
     up_ring.complete()
     for part in range(row_parts):
         expert(part, lax.rem(mt + 2, tp_count))
@@ -608,16 +653,17 @@
         out_ref[:, cols] = (stream_ref[:, cols].astype(F32) + mix).astype(BF16)
 
     for chunk in range(chunks):
-        down_rings[chunk].forward()
-        if chunk + 2 < chunks:
-            down_rings[chunk + 2].start()
+        if chunk:
+            down_rings[chunk].forward()
+            if chunk + 2 < chunks:
+                down_rings[chunk + 2].start()
         down_rings[chunk].complete()
         answer(chunk)
     for chunk in range(chunks):
         finish(chunk)
     left = send_ref.at[pl.ds(0, sp_count - 1)]
     whole(left, left, send5, recv5.at[0]).wait_send()
-    for ring in (gate_ring, up_ring, *down_rings):
+    for ring in (gate_ring, gate_rest, up_ring, *down_rings):
         ring.sent()
 
 
@@ -648,6 +694,7 @@
     hidden_part = gate_weight.shape[2]
     planes = sp_count // PLANE
     slots = sp_count * capacity
+    rows = head // PLANE
     dma = pltpu.SemaphoreType.DMA
     vmem = pltpu.VMEM
     return pl.pallas_call(
@@ -673,12 +720,16 @@
             vmem((tp_count, model, hidden_part), BF16),
             vmem((length, width), F32),
             vmem((length, width), F32),
-            vmem((PLANE, 16, width), F32),
-            vmem((PLANE, 16, width), F32),
-            vmem((1, 16, width), F32),
-            vmem((planes, 16, width), F32),
-            vmem((PLANE, 16, width), F32),
-            vmem((PLANE, 16, width), F32),
+            vmem((PLANE, rows, width), F32),
+            vmem((1, 2, width), F32),
+            vmem((PLANE, rows, width), F32),
+            vmem((PLANE, 2, width), F32),
+            vmem((1, rows, width), F32),
+            vmem((1, 2, width), F32),
+            vmem((planes, rows, width), F32),
+            vmem((planes, 2, width), F32),
+            vmem((PLANE, rows, width), F32),
+            vmem((PLANE, rows, width), F32),
             vmem((tp_count, tokens, width), BF16),
             vmem((tp_count, tokens, width), BF16),
             vmem((tokens, model), BF16),
@@ -695,11 +746,15 @@
             dma,
             dma,
             dma,
+            dma,
+            dma,
+            dma,
+            dma,
             dma((2,)),
             dma((len(WIDTHS),)),
             dma((len(WIDTHS),)),
-            dma((2 + len(WIDTHS), 4)),
-            dma((2 + len(WIDTHS), 4)),
+            dma((3 + len(WIDTHS), 4)),
+            dma((3 + len(WIDTHS), 4)),
             *[vmem((sp_count, capacity, n), BF16) for n in WIDTHS],
             *[vmem((sp_count, capacity, n), BF16) for n in WIDTHS],
             *[vmem((tp_count, hidden_part, n), BF16) for n in WIDTHS],

time: 150 us -> 143 us (0.953)
  Pallas kernels: 148 us -> 140 us
    pallas_call x1, Pallas kernels: 148 us -> 140 us  [shards(): pl.pallas_call(functools.partial(layer_kernel, sp_count, tp_count, head_c...]
where the time goes in v4:
time: 143 us; the launch traced here: 142 us
  Pallas kernels  140 us (98%)
  local copies, waits for them, and re-layouts  1.88 us (1%)
    pallas_call x1, Pallas kernels, shards(): pl.pallas_call(functools.partial(layer_kernel, sp_count, tp_count, head_c...  140 us

profile of v4, /device:TPU:1, one launch (start us, length us, event | category | flops | bytes accessed | tf_op | source)
XLA Modules:
  0.0 142.4 jit_solution(10755796298063723432)
XLA Ops:
  0.0 140.5 %shard_map.154 = bf16[128,2048]{1,0:T(8,128)(2,1)} custom-call(bf16[512,256]{1,0:T(8,128)(2,1)} %refs_0_.1, bf16[512,256]{1,0:T(8,128)(2,1)} %refs_1_.1, bf16[512,256]{1,0:T(8,128)(2,1)} %refs_2_.1, bf16[512,256]{1,0:T(8,128)(2,1)} %refs_3_.1, f32[4,512]{1,0:T(4,128)} %bitcast.6, f32[4,512]{1,0:T(4,128)} %bitcast.7, f32[4,64]{1,0:T(4,128)} %refs_6_.1, ...), custom_call_target="tpu_custom_call" | custom-call | tf_op jit(solution)/shard_map/pallas_call | solution.py:700
  140.5 1.9 %copy.18 = bf16[128,2048]{1,0:T(8,128)(2,1)} copy(bf16[128,2048]{1,0:T(8,128)(2,1)} %shard_map.154) | data formatting | bytes 1048576

commit v5 on v4

--- a/solution.py
+++ b/solution.py
@@ -607,7 +607,6 @@
         if part == 0:
             down_rings[0].forward()
             down_rings[1].start()
-            down_rings[2].start()
     gate_ring.complete()
     gate_rest.complete()
     up_ring.complete()
@@ -655,8 +654,8 @@
     for chunk in range(chunks):
         if chunk:
             down_rings[chunk].forward()
-            if chunk + 2 < chunks:
-                down_rings[chunk + 2].start()
+            if chunk + 1 < chunks:
+                down_rings[chunk + 1].start()
         down_rings[chunk].complete()
         answer(chunk)
     for chunk in range(chunks):

time: 143 us -> 142 us (level)
  no operation moved by 1% of the time
where the time goes in v5:
time: 142 us
  Pallas kernels  140 us (99%)
  local copies, waits for them, and re-layouts  1.88 us (1%)
    pallas_call x1, Pallas kernels, shards(): pl.pallas_call(functools.partial(layer_kernel, sp_count, tp_count, head_c...  140 us

profile of v5, /device:TPU:1, one launch (start us, length us, event | category | flops | bytes accessed | tf_op | source)
XLA Modules:
  0.0 141.6 jit_solution(15901806020120622360)
XLA Ops:
  0.0 139.7 %shard_map.154 = bf16[128,2048]{1,0:T(8,128)(2,1)} custom-call(bf16[512,256]{1,0:T(8,128)(2,1)} %refs_0_.1, bf16[512,256]{1,0:T(8,128)(2,1)} %refs_1_.1, bf16[512,256]{1,0:T(8,128)(2,1)} %refs_2_.1, bf16[512,256]{1,0:T(8,128)(2,1)} %refs_3_.1, f32[4,512]{1,0:T(4,128)} %bitcast.6, f32[4,512]{1,0:T(4,128)} %bitcast.7, f32[4,64]{1,0:T(4,128)} %refs_6_.1, ...), custom_call_target="tpu_custom_call" | custom-call | tf_op jit(solution)/shard_map/pallas_call | solution.py:699
  139.7 1.9 %copy.18 = bf16[128,2048]{1,0:T(8,128)(2,1)} copy(bf16[128,2048]{1,0:T(8,128)(2,1)} %shard_map.154) | data formatting | bytes 1048576

commit v6 on v5

--- a/solution.py
+++ b/solution.py
@@ -11,7 +11,7 @@
 VERY_NEGATIVE = -1e30
 MESH = pl.DeviceIdType.MESH
 PLANE = 8
-WIDTHS = (256, 256, 256, 256, 512, 512)
+WIDTHS = (256, 256, 384, 384, 384, 384)
 F32 = jnp.float32
 BF16 = jnp.bfloat16
 
@@ -613,8 +613,6 @@
     for part in range(row_parts):
         expert(part, lax.rem(mt + 2, tp_count))
 
-    wide = 256
-
     def give(chunk, step):
         peer = ring_source(me, step, sp_count)
         return pltpu.make_async_remote_copy(
@@ -628,6 +626,7 @@
 
     def answer(chunk):
         down_ref, back_ref = down_refs[chunk], back_refs[chunk]
+        wide = 384 if WIDTHS[chunk] == 384 else 256
         for n in range(WIDTHS[chunk] // wide):
             cols = slice(n * wide, (n + 1) * wide)
             result = jnp.zeros((slots, wide), F32)

time: 142 us -> 141 us (level)
  no operation moved by 1% of the time
where the time goes in v6:
time: 141 us
  Pallas kernels  139 us (99%)
  local copies, waits for them, and re-layouts  1.88 us (1%)
    pallas_call x1, Pallas kernels, shards(): pl.pallas_call(functools.partial(layer_kernel, sp_count, tp_count, head_c...  139 us

profile of v6, /device:TPU:1, one launch (start us, length us, event | category | flops | bytes accessed | tf_op | source)
XLA Modules:
  0.0 141.1 jit_solution(12072047429511081056)
XLA Ops:
  0.0 139.2 %shard_map.154 = bf16[128,2048]{1,0:T(8,128)(2,1)} custom-call(bf16[512,256]{1,0:T(8,128)(2,1)} %refs_0_.1, bf16[512,256]{1,0:T(8,128)(2,1)} %refs_1_.1, bf16[512,256]{1,0:T(8,128)(2,1)} %refs_2_.1, bf16[512,256]{1,0:T(8,128)(2,1)} %refs_3_.1, f32[4,512]{1,0:T(4,128)} %bitcast.6, f32[4,512]{1,0:T(4,128)} %bitcast.7, f32[4,64]{1,0:T(4,128)} %refs_6_.1, ...), custom_call_target="tpu_custom_call" | custom-call | tf_op jit(solution)/shard_map/pallas_call | solution.py:698
  139.2 1.9 %copy.18 = bf16[128,2048]{1,0:T(8,128)(2,1)} copy(bf16[128,2048]{1,0:T(8,128)(2,1)} %shard_map.154) | data formatting | bytes 1048576
